TPU v7x, 512 devices: a whole 4x8x8 slice. The times are simulated.
512 devices in a mesh: dp: 4 (over x), kv: 64 (over z, y), tp: 2 (over core).
Axes of the slice: x: 4, y: 8, z: 8, core: 2. Of those that a mesh axis runs over, the one named last changes fastest.
Arguments:
- hidden: bfloat16 [2048, 256], P(('kv', 'tp'), 'dp'), parts along dimension 1, may hold values from -20 to 20
- mixer_gain: float32 [2048], replicated, may hold values from 0.1 to 1.9
- gate_proj: bfloat16 [2048, 64, 64], P(None, 'kv', 'tp'), may hold values from -0.125 to 0.125
- inner_proj: bfloat16 [2048, 64, 64], P(None, 'kv', 'tp'), may hold values from -0.125 to 0.125
- input_proj: bfloat16 [2048, 1024], P(None, 'kv'), may hold values from -0.125 to 0.125
- output_proj: bfloat16 [2048, 1024], P(None, 'kv'), may hold values from -0.125 to 0.125
- step_proj: bfloat16 [2048, 64], replicated, may hold values from -0.125 to 0.125
- step_bias: float32 [64], replicated, may hold values from -3 to -0.5
- decay_log: float32 [64], replicated, may hold values from -3 to 1
- skip_gain: float32 [64], replicated, may hold values from 0.3 to 1.5
- taps_inner: float32 [4, 64, 64], P(None, None, 'tp'), may hold values from -3 to 3
- taps_input: float32 [4, 1024], replicated, may hold values from -3 to 3
- taps_output: float32 [4, 1024], replicated, may hold values from -3 to 3
- recent_inner: bfloat16 [256, 3, 64, 64], P(('dp', 'kv'), None, None, 'tp'), parts along dimension 0, may hold values from -6 to 6
- recent_input: bfloat16 [256, 3, 1024], P(('dp', 'kv')), parts along dimension 0, may hold values from -6 to 6
- recent_output: bfloat16 [256, 3, 1024], P(('dp', 'kv')), parts along dimension 0, may hold values from -6 to 6
- states: float32 [256, 64, 64, 128], P(('dp', 'kv'), None, 'tp'), parts along dimension 0, may hold values from -4 to 4
- block_inner: bfloat16 [256, 128, 64, 64], P(('dp', 'kv'), None, None, 'tp'), parts along dimension 0, may hold values from -6 to 6
- block_input: bfloat16 [256, 128, 1024], P(('dp', 'kv')), parts along dimension 0, may hold values from -4 to 4
- block_decay: float32 [256, 128, 64], P(('dp', 'kv')), parts along dimension 0
- lengths: int32 [256], P(('dp', 'kv')), parts along dimension 0, may hold values from 1 to 128, 2730 in all
- norm_gain: float32 [64, 64], P(None, 'tp'), may hold values from 0.1 to 1.9
- mixer_out: bfloat16 [64, 64, 2048], P('kv', 'tp'), may hold values from -0.25 to 0.25
- channel_gain: float32 [2048], replicated, may hold values from 0.1 to 1.9
- expand_gate: bfloat16 [2048, 5632], P(None, ('kv', 'tp')), may hold values from -0.125 to 0.125
- expand_value: bfloat16 [2048, 5632], P(None, ('kv', 'tp')), may hold values from -0.125 to 0.125
- reduce_proj: bfloat16 [5632, 2048], P(('kv', 'tp')), may hold values from -0.3125 to 0.3125
Outputs:
- layer_out: bfloat16 [2048, 256], P(('kv', 'tp'), 'dp'), parts along dimension 1
There are 4 independent parts, one for each index of `dp`. A program takes and returns all parts, laid end to end along the dimension named above; an argument that names none is the same for every part. Nothing has to cross between parts.
All inputs are finite; a program needn't handle non-finite values. No bound on the sum of `lengths` on one device may be relied on, other than what follows from the above.
Results may differ from a plain program's by a relative error of at most 0.01.
Values may be sent and summed in bfloat16 or wider, within the bound.
A program may use at most 64 MiB of HBM per device.

v0:
```python
import jax
import jax.numpy as jnp
from jax import lax
from jax.sharding import Mesh
from jax.sharding import PartitionSpec as P

MIXER_HEADS = 64
HEAD_DIM = 64
GROUPS = 8
STATE = 128
OPEN_BLOCK_SPAN = 128
KV = ("kv_0", "kv_1")
KV_TP = ("kv_0", "kv_1", "tp")
DP_KV = ("dp", "kv_0", "kv_1")


epsilon = 1e-05


def from_everyone(value, axis):
    length = lax.axis_size(axis)
    return lax.all_to_all(
        jnp.broadcast_to(value[None], (length, *value.shape)), axis, 0, 0, tiled=True
    )


def in_order(blocks, dim):
    shape = list(blocks.shape[1:])
    shape[dim] *= blocks.shape[0]
    return jnp.moveaxis(blocks, 0, dim).reshape(shape)


def gathered_by_axis(value, axes, dim):
    far, near = axes
    blocks = from_everyone(from_everyone(value, far), near)
    return in_order(blocks.swapaxes(0, 1).reshape(-1, *value.shape), dim)


def sent_together(arrays, axis, split_dim, concat_dim, along):
    ends, at = ([], 0)
    for a in arrays[:-1]:
        at += a.shape[along]
        ends.append(at)
    both = jnp.concatenate(arrays, axis=along)
    return tuple(
        jnp.split(
            lax.all_to_all(both, axis, split_axis=split_dim, concat_axis=concat_dim, tiled=True),
            ends,
            axis=along,
        )
    )


def of_everyone(value, axis):
    everything = from_everyone(value, axis)
    return jnp.sum(everything, axis=0)


def by_axis(value, axes):
    far, near = axes
    return of_everyone(of_everyone(value, near), far)


def padded_to(lines, length):
    spare = -len(lines) % length
    return jnp.pad(lines, [(0, spare)] + [(0, 0)] * (lines.ndim - 1))


def in_blocks(value, dim, length):
    shape = value.shape
    blocks = value.reshape(*shape[:dim], length, shape[dim] // length, *shape[dim + 1 :])
    return jnp.moveaxis(blocks, dim, 0)


def sent_and_summed(value, axis, dim):
    blocks = in_blocks(value, dim, lax.axis_size(axis))
    arrived = lax.all_to_all(blocks, axis, split_axis=0, concat_axis=0, tiled=True)
    return arrived.astype(jnp.float32).sum(axis=0)


def sum_in_two_steps(value, axes, dim):
    far, near = axes
    own = sent_and_summed(in_blocks(value, dim, lax.axis_size(far)), near, dim + 1)
    return jnp.sum(
        lax.all_to_all(own.astype(jnp.bfloat16), far, 0, 0, tiled=True).astype(jnp.float32), axis=0
    )


def sum_by_parts(value, axes):
    lines = value.reshape(-1, value.shape[-1])
    padded = padded_to(lines, lax.axis_size(axes[0]) * lax.axis_size(axes[1]))
    whole = gathered_by_axis(sum_in_two_steps(padded, axes, 0).astype(jnp.bfloat16), axes, 0)
    return lax.slice_in_dim(whole, 0, len(lines)).reshape(value.shape).astype(jnp.float32)


def summed_on_arrival(value, axis, dim):
    length = lax.axis_size(axis)
    blocks = lax.all_to_all(in_blocks(value, dim, length), axis, 0, 0, tiled=True)
    return jnp.sum(blocks, axis=0)


def summed_rows(value, axes, dim):
    far, near = axes
    blocks = in_blocks(value, dim, lax.axis_size(far))
    nearer = summed_on_arrival(blocks, near, dim + 1)
    arrived = lax.all_to_all(nearer, far, split_axis=0, concat_axis=0, tiled=True)
    return arrived.sum(axis=0)


def short_conv(recent, newest, taps):
    window = jnp.concatenate(
        [recent.astype(jnp.float32), newest.astype(jnp.float32)[:, None]], axis=1
    )
    return jax.nn.silu(jnp.sum(window * taps[None], axis=1))


def shards(
    hidden,
    mixer_gain,
    gate_proj,
    inner_proj,
    input_proj,
    output_proj,
    step_proj,
    step_bias,
    decay_log,
    skip_gain,
    taps_inner,
    taps_input,
    taps_output,
    recent_inner,
    recent_input,
    recent_output,
    states,
    block_inner,
    block_input,
    block_decay,
    lengths,
    norm_gain,
    mixer_out,
    channel_gain,
    expand_gate,
    expand_value,
    reduce_proj,
):
    rows_own = hidden.shape[0]
    seq_all = hidden.shape[1]
    seq_dev = states.shape[0]
    half_dim = states.shape[2]
    width = rows_own * lax.axis_size(KV) * lax.axis_size("tp")
    offset = (lax.axis_index(KV) * lax.axis_size("tp") + lax.axis_index("tp")) * rows_own
    own_start = lax.axis_index(KV) * seq_dev
    whole_rows = gathered_by_axis(hidden, (("kv_0", "kv_1"), "tp"), 0)
    whole_f = whole_rows.astype(jnp.float32)
    rms_in = lax.rsqrt(jnp.mean(whole_f * whole_f, axis=0) + epsilon)
    normed_in = (whole_f * mixer_gain[:, None]).astype(jnp.bfloat16)
    gate_part = (
        rms_in[:, None, None]
        * jnp.einsum("ds,dhp->shp", normed_in, gate_proj, preferred_element_type=jnp.float32)
    ).astype(jnp.bfloat16)
    inner_part = (
        rms_in[:, None, None]
        * jnp.einsum("ds,dhp->shp", normed_in, inner_proj, preferred_element_type=jnp.float32)
    ).astype(jnp.bfloat16)
    input_part = (
        rms_in[:, None]
        * jnp.einsum("ds,dk->sk", normed_in, input_proj, preferred_element_type=jnp.float32)
    ).astype(jnp.bfloat16)
    output_part = (
        rms_in[:, None]
        * jnp.einsum("ds,dk->sk", normed_in, output_proj, preferred_element_type=jnp.float32)
    ).astype(jnp.bfloat16)
    own_cols = lax.dynamic_slice_in_dim(normed_in, own_start, seq_dev, 1)
    own_rms = lax.dynamic_slice_in_dim(rms_in, own_start, seq_dev, 0)
    step_pre = (
        own_rms[:, None]
        * jnp.einsum("ds,dh->sh", own_cols, step_proj, preferred_element_type=jnp.float32)
    ).astype(jnp.bfloat16)
    gate_pre, inner_pre, input_pre, output_pre = (
        *sent_together((gate_part, inner_part), KV, 0, 1, 2),
        lax.all_to_all(input_part, KV, split_axis=0, concat_axis=1, tiled=True),
        lax.all_to_all(output_part, KV, split_axis=0, concat_axis=1, tiled=True),
    )
    conv_inner = short_conv(recent_inner, inner_pre, taps_inner)
    conv_input = short_conv(recent_input, input_pre, taps_input)
    conv_output = short_conv(recent_output, output_pre, taps_output).astype(jnp.bfloat16)
    step = jax.nn.softplus(step_pre.astype(jnp.float32) + step_bias[None, :])
    new_decay = -jnp.exp(decay_log)[None, :] * step
    per_group = MIXER_HEADS // GROUPS
    live = (jnp.arange(OPEN_BLOCK_SPAN, dtype=jnp.int32)[None, :] < lengths[:, None]).astype(
        jnp.float32
    )
    masked = block_decay * live[:, :, None]
    cached = jnp.sum(masked, axis=1)
    tail = new_decay[:, None, :] + cached[:, None, :] - jnp.cumsum(masked, axis=1)
    total = new_decay + cached
    readout = conv_output.reshape(seq_dev, GROUPS, STATE)
    score = jnp.einsum(
        "sgn,sjgn->sgj",
        readout,
        block_input.reshape(seq_dev, OPEN_BLOCK_SPAN, GROUPS, STATE),
        preferred_element_type=jnp.float32,
    )
    score_heads = jnp.repeat(score, per_group, axis=1)
    weight = (live[:, None, :] * jnp.exp(jnp.swapaxes(tail, 1, 2)) * score_heads).astype(
        jnp.bfloat16
    )
    from_block = jnp.einsum(
        "shj,sjhp->shp", weight, block_inner, preferred_element_type=jnp.float32
    )
    readout_f = readout.astype(jnp.float32)
    grouped = states.reshape(seq_dev, GROUPS, per_group, half_dim, STATE)
    from_state = jnp.einsum(
        "sgn,sgrpn->sgrp", readout_f, grouped, precision=lax.Precision.HIGHEST
    ).reshape(seq_dev, MIXER_HEADS, half_dim)
    own_score = jnp.repeat(
        jnp.sum(readout_f * conv_input.reshape(seq_dev, GROUPS, STATE), axis=-1), per_group, axis=1
    )
    mix = (
        from_block
        + jnp.exp(total)[:, :, None] * from_state
        + (own_score * step)[:, :, None] * conv_inner
        + skip_gain[None, :, None] * conv_inner
    )
    gated_raw = mix * jax.nn.silu(gate_pre.astype(jnp.float32))
    part_squares = jnp.sum(gated_raw * gated_raw, axis=(1, 2))
    gated = (gated_raw * norm_gain[None]).astype(jnp.bfloat16)
    placed = lax.dynamic_update_slice_in_dim(
        jnp.zeros((seq_all,), jnp.float32), part_squares, own_start, 0
    )
    gate_squares = by_axis(placed, (("kv_0", "kv_1"), "tp"))
    rms_gate = lax.rsqrt(gate_squares / (MIXER_HEADS * HEAD_DIM) + epsilon)
    by_head = lax.all_to_all(gated, KV, split_axis=1, concat_axis=0, tiled=True)
    columns = mixer_out
    mixed_full = rms_gate[None, :] * sum_by_parts(
        jnp.einsum("hpd,shp->ds", columns, by_head, preferred_element_type=jnp.float32).astype(
            jnp.bfloat16
        ),
        (("kv_0", "kv_1"), "tp"),
    )
    mid_full = (whole_f + mixed_full).astype(jnp.bfloat16)
    mid = lax.dynamic_slice_in_dim(mid_full, offset, rows_own, 0)
    full_f = mid_full.astype(jnp.float32)
    mid_squares = jnp.sum(full_f * full_f, axis=0)
    normed_full = (full_f * channel_gain[:, None]).astype(jnp.bfloat16)
    gate_sum = jnp.einsum("ds,df->sf", normed_full, expand_gate, preferred_element_type=jnp.float32)
    value_sum = jnp.einsum(
        "ds,df->sf", normed_full, expand_value, preferred_element_type=jnp.float32
    )
    rms_mid = lax.rsqrt(mid_squares / width + epsilon)
    act = (jax.nn.silu(rms_mid[:, None] * gate_sum) * (rms_mid[:, None] * value_sum)).astype(
        jnp.bfloat16
    )
    columns = reduce_proj
    channel = summed_rows(
        jnp.einsum("fd,sf->ds", columns, act, preferred_element_type=jnp.float32),
        (("kv_0", "kv_1"), "tp"),
        0,
    )
    return (mid.astype(jnp.float32) + channel).astype(jnp.bfloat16)


def solution(mesh):
    finer = Mesh(
        mesh.devices.reshape(mesh.shape["dp"], 8, 8, mesh.shape["tp"]), ("dp", "kv_0", "kv_1", "tp")
    )
    in_specs = (
        P(KV_TP, "dp"),
        P(),
        P(None, KV, "tp"),
        P(None, KV, "tp"),
        P(None, KV),
        P(None, KV),
        P(),
        P(),
        P(),
        P(),
        P(None, None, "tp"),
        P(),
        P(),
        P(DP_KV, None, None, "tp"),
        P(DP_KV, None, None),
        P(DP_KV, None, None),
        P(DP_KV, None, "tp", None),
        P(DP_KV, None, None, "tp"),
        P(DP_KV, None, None),
        P(DP_KV, None, None),
        P(DP_KV),
        P(None, "tp"),
        P(KV, "tp", None),
        P(),
        P(None, KV_TP),
        P(None, KV_TP),
        P(KV_TP, None),
    )
    out_specs = P(KV_TP, "dp")
    return jax.shard_map(
        shards, mesh=finer, in_specs=in_specs, out_specs=out_specs, check_vma=False
    )
```

profile of v0, /device:TPU:1, one launch (start us, length us, event | category | flops | bytes accessed | tf_op | source)
XLA Modules:
  0.0 220.0 jit_solution(13362127594896398965)
XLA Ops:
  1.7 17.3 %all-to-all-start = ((bf16[64,2,512]{2,1,0:T(2,128)(2,1)}), bf16[64,2,512]{2,1,0:T(2,128)(2,1)S(1)}, u32[]{:S(2)}, u32[]{:S(2)}) async-start(bf16[64,2,512]{2,1,0:T(2,128)(2,1)} %reshape.425), calls=%async_computation | async-start | bytes 262144 | tf_op jit(solution)/shard_map/all_to_all | solution.py:22
  21.5 9.0 %all-to-all-done = bf16[64,2,512]{2,1,0:T(2,128)(2,1)S(1)} async-done(((bf16[64,2,512]{2,1,0:T(2,128)(2,1)}), bf16[64,2,512]{2,1,0:T(2,128)(2,1)S(1)}, u32[]{:S(2)}, u32[]{:S(2)}) %all-to-all-start) | async-done | bytes 131104 | tf_op jit(solution)/shard_map/all_to_all | solution.py:22
  31.2 5.7 %all_to_all.99 = bf16[2,2,32768]{2,1,0:T(2,128)(2,1)S(1)} all-to-all(bf16[2,2,32768]{2,1,0:T(2,128)(2,1)S(1)} %reshape.427), channel_id=1, replica_groups=mesh['dp'=4,'kv_0'=8,'kv_1'=8,'tp'=2] {'tp'}, dimensions={0} | all-to-all | bytes 524288 | tf_op jit(solution)/shard_map/all_to_all | solution.py:22
  37.7 0.9 copy-done.7
  42.4 4.6 %all-to-all-start.3 = ((bf16[64,1,16]{2,1,0:T(2,128)(2,1)}), bf16[64,1,16]{2,1,0:T(2,128)(2,1)S(1)}, u32[]{:S(2)}, u32[]{:S(2)}) async-start(bf16[64,1,16]{2,1,0:T(2,128)(2,1)} %copy.107), calls=%async_computation.3 | async-start | bytes 65536 | tf_op jit(solution)/shard_map/all_to_all | solution.py:181
  47.8 10.1 %all-to-all-done.3 = bf16[64,1,16]{2,1,0:T(2,128)(2,1)S(1)} async-done(((bf16[64,1,16]{2,1,0:T(2,128)(2,1)}), bf16[64,1,16]{2,1,0:T(2,128)(2,1)S(1)}, u32[]{:S(2)}, u32[]{:S(2)}) %all-to-all-start.3) | async-done | bytes 2080 | tf_op jit(solution)/shard_map/all_to_all | solution.py:181
  57.9 4.6 %all-to-all-start.2 = ((bf16[64,1,16]{2,1,0:T(2,128)(2,1)}), bf16[64,1,16]{2,1,0:T(2,128)(2,1)S(1)}, u32[]{:S(2)}, u32[]{:S(2)}) async-start(bf16[64,1,16]{2,1,0:T(2,128)(2,1)} %copy.104), calls=%async_computation.2 | async-start | bytes 65536 | tf_op jit(solution)/shard_map/all_to_all | solution.py:182
  62.5 1.0 dynamic-slice_reduce_fusion
  65.0 8.4 %all-to-all-done.2 = bf16[64,1,16]{2,1,0:T(2,128)(2,1)S(1)} async-done(((bf16[64,1,16]{2,1,0:T(2,128)(2,1)}), bf16[64,1,16]{2,1,0:T(2,128)(2,1)S(1)}, u32[]{:S(2)}, u32[]{:S(2)}) %all-to-all-start.2) | async-done | bytes 2080 | tf_op jit(solution)/shard_map/all_to_all | solution.py:182
  73.4 4.6 %all-to-all-start.4 = ((bf16[64,1,64]{2,1,0:T(2,128)(2,1)}), bf16[64,1,64]{2,1,0:T(2,128)(2,1)S(1)}, u32[]{:S(2)}, u32[]{:S(2)}) async-start(bf16[64,1,64]{2,1,0:T(2,128)(2,1)} %copy.110), calls=%async_computation.4 | async-start | bytes 65536 | tf_op jit(solution)/shard_map/all_to_all | solution.py:47
  81.8 2.1 fusion.50
  84.4 4.4 %all-to-all-done.4 = bf16[64,1,64]{2,1,0:T(2,128)(2,1)S(1)} async-done(((bf16[64,1,64]{2,1,0:T(2,128)(2,1)}), bf16[64,1,64]{2,1,0:T(2,128)(2,1)S(1)}, u32[]{:S(2)}, u32[]{:S(2)}) %all-to-all-start.4) | async-done | bytes 8224 | tf_op jit(solution)/shard_map/all_to_all | solution.py:47
  91.7 7.7 %all-to-all-start.7 = ((bf16[1,64,32]{2,0,1:T(2,128)(2,1)}), bf16[1,64,32]{2,0,1:T(2,128)(2,1)S(1)}, u32[]{:S(2)}, u32[]{:S(2)}) async-start(bf16[1,64,32]{2,0,1:T(2,128)(2,1)} %copy.115), calls=%async_computation.7 | async-start | bytes 65536 | tf_op jit(solution)/shard_map/all_to_all | solution.py:233
  100.2 10.1 %all-to-all-done.7 = bf16[1,64,32]{2,0,1:T(2,128)(2,1)S(1)} async-done(((bf16[1,64,32]{2,0,1:T(2,128)(2,1)}), bf16[1,64,32]{2,0,1:T(2,128)(2,1)S(1)}, u32[]{:S(2)}, u32[]{:S(2)}) %all-to-all-start.7) | async-done | bytes 4128 | tf_op jit(solution)/shard_map/all_to_all | solution.py:233
  111.8 1.4 reshape.429
  113.2 8.2 %all_to_all.100 = bf16[2,2,32768]{2,1,0:T(2,128)(2,1)S(1)} all-to-all(bf16[2,2,32768]{2,1,0:T(2,128)(2,1)S(1)} %reshape.429), channel_id=1, replica_groups=mesh['dp'=4,'kv_0'=8,'kv_1'=8,'tp'=2] {'tp'}, dimensions={0} | all-to-all | bytes 524288 | tf_op jit(solution)/shard_map/all_to_all | solution.py:77
  121.9 3.5 %all-to-all-start.5 = ((f32[2,1,64]{2,1,0:T(1,128)}), f32[2,1,64]{2,1,0:T(1,128)S(1)}, u32[]{:S(2)}, u32[]{:S(2)}) async-start(f32[2,1,64]{2,1,0:T(1,128)} %broadcast_in_dim.28), calls=%async_computation.5 | async-start | bytes 2048 | tf_op jit(solution)/shard_map/all_to_all | solution.py:22
  126.9 4.6 %all-to-all-start.9 = ((bf16[64,2,512]{2,1,0:T(2,128)(2,1)}), bf16[64,2,512]{2,1,0:T(2,128)(2,1)S(1)}, u32[]{:S(2)}, u32[]{:S(2)}) async-start(bf16[64,2,512]{2,1,0:T(2,128)(2,1)} %reshape.431), calls=%async_computation.9 | async-start | bytes 262144 | tf_op jit(solution)/shard_map/all_to_all | solution.py:85
  131.5 11.9 %all-to-all-done.9 = bf16[64,2,512]{2,1,0:T(2,128)(2,1)S(1)} async-done(((bf16[64,2,512]{2,1,0:T(2,128)(2,1)}), bf16[64,2,512]{2,1,0:T(2,128)(2,1)S(1)}, u32[]{:S(2)}, u32[]{:S(2)}) %all-to-all-start.9) | async-done | bytes 131104 | tf_op jit(solution)/shard_map/all_to_all | solution.py:85
  144.1 4.5 %all-to-all-start.6 = ((f32[64,1,64]{2,1,0:T(1,128)}), f32[64,1,64]{2,1,0:T(1,128)S(1)}, u32[]{:S(2)}, u32[]{:S(2)}) async-start(f32[64,1,64]{2,1,0:T(1,128)} %broadcast_in_dim.29), calls=%async_computation.6 | async-start | bytes 65536 | tf_op jit(solution)/shard_map/all_to_all | solution.py:22
  149.8 9.7 %all-to-all-done.6 = f32[64,1,64]{2,1,0:T(1,128)S(1)} async-done(((f32[64,1,64]{2,1,0:T(1,128)}), f32[64,1,64]{2,1,0:T(1,128)S(1)}, u32[]{:S(2)}, u32[]{:S(2)}) %all-to-all-start.6) | async-done | bytes 16416 | tf_op jit(solution)/shard_map/all_to_all | solution.py:22
  159.5 4.6 %all-to-all-start.10 = ((bf16[64,2,512]{2,1,0:T(2,128)(2,1)}), bf16[64,2,512]{2,1,0:T(2,128)(2,1)S(1)}, u32[]{:S(2)}, u32[]{:S(2)}) async-start(bf16[64,2,512]{2,1,0:T(2,128)(2,1)} %reshape.433), calls=%async_computation.10 | async-start | bytes 262144 | tf_op jit(solution)/shard_map/all_to_all | solution.py:22
  164.1 11.5 %all-to-all-done.10 = bf16[64,2,512]{2,1,0:T(2,128)(2,1)S(1)} async-done(((bf16[64,2,512]{2,1,0:T(2,128)(2,1)}), bf16[64,2,512]{2,1,0:T(2,128)(2,1)S(1)}, u32[]{:S(2)}, u32[]{:S(2)}) %all-to-all-start.10) | async-done | bytes 131104 | tf_op jit(solution)/shard_map/all_to_all | solution.py:22
  176.4 8.2 %all_to_all.101 = bf16[2,2,32768]{2,1,0:T(2,128)(2,1)} all-to-all(bf16[2,2,32768]{2,1,0:T(2,128)(2,1)S(1)} %reshape.435), channel_id=1, replica_groups=mesh['dp'=4,'kv_0'=8,'kv_1'=8,'tp'=2] {'tp'}, dimensions={0} | all-to-all | bytes 524288 | tf_op jit(solution)/shard_map/all_to_all | solution.py:22
  184.5 1.3 reshape.436
  190.4 4.1 %all_to_all.102 = f32[2,1,65536]{2,1,0:T(1,128)S(1)} all-to-all(f32[2,1,65536]{2,1,0:T(1,128)S(1)} %reshape.437), channel_id=1, replica_groups=mesh['dp'=4,'kv_0'=8,'kv_1'=8,'tp'=2] {'tp'}, dimensions={0} | all-to-all | bytes 1048576 | tf_op jit(solution)/shard_map/all_to_all | solution.py:98
  195.1 2.3 %reduce.21 = f32[2,65536]{1,0:T(2,128)S(1)} reduce(f32[2,1,65536]{2,1,0:T(1,128)S(1)} %all_to_all.102, f32[]{:T(128)} %broadcast.194), dimensions={1}, to_apply=%all_to_all.83.reduce_sub_computation | reduce | bytes 1048580 | tf_op jit(solution)/shard_map/all_to_all | solution.py:98
  198.1 1.0 reshape.439
  199.2 4.6 %all-to-all-start.13 = ((f32[64,1,1024]{2,1,0:T(1,128)}), f32[64,1,1024]{2,1,0:T(1,128)S(1)}, u32[]{:S(2)}, u32[]{:S(2)}) async-start(f32[64,1,1024]{2,1,0:T(1,128)} %reshape.439), calls=%async_computation.13 | async-start | bytes 524288 | tf_op jit(solution)/shard_map/all_to_all | solution.py:106
  203.8 13.4 %all-to-all-done.13 = f32[64,1,1024]{2,1,0:T(1,128)S(1)} async-done(((f32[64,1,1024]{2,1,0:T(1,128)}), f32[64,1,1024]{2,1,0:T(1,128)S(1)}, u32[]{:S(2)}, u32[]{:S(2)}) %all-to-all-start.13) | async-done | bytes 262176 | tf_op jit(solution)/shard_map/all_to_all | solution.py:106
  217.2 1.3 reduce.22
  218.7 1.3 add_convert_fusion
  (155 shorter events, 30.7 us)
Async XLA Ops:
  0.0 81.8 %copy-start = (f32[1,64,32,128]{3,2,1,0:T(8,128)S(1)}, f32[1,64,32,128]{3,2,1,0:T(8,128)}, u32[]{:S(2)}) copy-start(f32[1,64,32,128]{3,2,1,0:T(8,128)} %param.43) | copy-start | bytes 3145732
  0.8 18.8 %copy-start.13 = (f32[1,128,64]{1,2,0:T(8,128)S(1)}, f32[1,128,64]{1,2,0:T(8,128)}, u32[]{:S(2)}) copy-start(f32[1,128,64]{1,2,0:T(8,128)} %param.46) | copy-start | bytes 98308
  1.7 18.8 %copy-start.3 = (bf16[1,128,1024]{2,1,0:T(8,128)(2,1)S(1)}, bf16[1,128,1024]{2,1,0:T(8,128)(2,1)}, u32[]{:S(2)}) copy-start(bf16[1,128,1024]{2,1,0:T(8,128)(2,1)} %param.45) | copy-start | bytes 786436
  1.7 28.8 %all-to-all-start = ((bf16[64,2,512]{2,1,0:T(2,128)(2,1)}), bf16[64,2,512]{2,1,0:T(2,128)(2,1)S(1)}, u32[]{:S(2)}, u32[]{:S(2)}) async-start(bf16[64,2,512]{2,1,0:T(2,128)(2,1)} %reshape.425), calls=%async_computation | async-start | bytes 262144 | tf_op jit(solution)/shard_map/all_to_all | solution.py:22
  19.6 1.1 copy-start.24
  37.7 3.2 %copy-start.22 = (f32[64]{0:T(128)}, f32[64]{0:T(128)S(1)}, u32[]{:S(2)}) copy-start(f32[64]{0:T(128)S(1)} %add_rsqrt_fusion.2) | copy-start | bytes 772
  37.7 0.9 copy-start.7
  38.6 0.9 copy-start.8
  39.8 0.9 copy-start.10
  40.7 0.8 copy-start.11
  42.4 15.5 %all-to-all-start.3 = ((bf16[64,1,16]{2,1,0:T(2,128)(2,1)}), bf16[64,1,16]{2,1,0:T(2,128)(2,1)S(1)}, u32[]{:S(2)}, u32[]{:S(2)}) async-start(bf16[64,1,16]{2,1,0:T(2,128)(2,1)} %copy.107), calls=%async_computation.3 | async-start | bytes 65536 | tf_op jit(solution)/shard_map/all_to_all | solution.py:181
  57.9 15.5 %all-to-all-start.2 = ((bf16[64,1,16]{2,1,0:T(2,128)(2,1)}), bf16[64,1,16]{2,1,0:T(2,128)(2,1)S(1)}, u32[]{:S(2)}, u32[]{:S(2)}) async-start(bf16[64,1,16]{2,1,0:T(2,128)(2,1)} %copy.104), calls=%async_computation.2 | async-start | bytes 65536 | tf_op jit(solution)/shard_map/all_to_all | solution.py:182
  62.5 1.0 copy-start.23
  73.4 15.5 %all-to-all-start.4 = ((bf16[64,1,64]{2,1,0:T(2,128)(2,1)}), bf16[64,1,64]{2,1,0:T(2,128)(2,1)S(1)}, u32[]{:S(2)}, u32[]{:S(2)}) async-start(bf16[64,1,64]{2,1,0:T(2,128)(2,1)} %copy.110), calls=%async_computation.4 | async-start | bytes 65536 | tf_op jit(solution)/shard_map/all_to_all | solution.py:47
  78.0 0.7 copy-start.18
  78.1 0.7 copy-start.17
  78.2 1.3 copy-start.28
  81.8 2.1 copy-start.2
  88.8 0.8 copy-start.9
  88.9 0.8 copy-start.14
  89.7 1.3 copy-start.16
  90.4 20.0 %copy-start.6 = (bf16[1,32,2048]{2,1,0:T(8,128)(2,1)S(1)}, bf16[1,32,2048]{2,1,0:T(8,128)(2,1)}, u32[]{:S(2)}) copy-start(bf16[1,32,2048]{2,1,0:T(8,128)(2,1)} %param.49) | copy-start | bytes 393220
  91.7 18.6 %all-to-all-start.7 = ((bf16[1,64,32]{2,0,1:T(2,128)(2,1)}), bf16[1,64,32]{2,0,1:T(2,128)(2,1)S(1)}, u32[]{:S(2)}, u32[]{:S(2)}) async-start(bf16[1,64,32]{2,0,1:T(2,128)(2,1)} %copy.115), calls=%async_computation.7 | async-start | bytes 65536 | tf_op jit(solution)/shard_map/all_to_all | solution.py:233
  121.9 5.0 %all-to-all-start.5 = ((f32[2,1,64]{2,1,0:T(1,128)}), f32[2,1,64]{2,1,0:T(1,128)S(1)}, u32[]{:S(2)}, u32[]{:S(2)}) async-start(f32[2,1,64]{2,1,0:T(1,128)} %broadcast_in_dim.28), calls=%async_computation.5 | async-start | bytes 2048 | tf_op jit(solution)/shard_map/all_to_all | solution.py:22
  126.9 16.6 %all-to-all-start.9 = ((bf16[64,2,512]{2,1,0:T(2,128)(2,1)}), bf16[64,2,512]{2,1,0:T(2,128)(2,1)S(1)}, u32[]{:S(2)}, u32[]{:S(2)}) async-start(bf16[64,2,512]{2,1,0:T(2,128)(2,1)} %reshape.431), calls=%async_computation.9 | async-start | bytes 262144 | tf_op jit(solution)/shard_map/all_to_all | solution.py:85
  144.1 15.4 %all-to-all-start.6 = ((f32[64,1,64]{2,1,0:T(1,128)}), f32[64,1,64]{2,1,0:T(1,128)S(1)}, u32[]{:S(2)}, u32[]{:S(2)}) async-start(f32[64,1,64]{2,1,0:T(1,128)} %broadcast_in_dim.29), calls=%async_computation.6 | async-start | bytes 65536 | tf_op jit(solution)/shard_map/all_to_all | solution.py:22
  159.5 16.2 %all-to-all-start.10 = ((bf16[64,2,512]{2,1,0:T(2,128)(2,1)}), bf16[64,2,512]{2,1,0:T(2,128)(2,1)S(1)}, u32[]{:S(2)}, u32[]{:S(2)}) async-start(bf16[64,2,512]{2,1,0:T(2,128)(2,1)} %reshape.433), calls=%async_computation.10 | async-start | bytes 262144 | tf_op jit(solution)/shard_map/all_to_all | solution.py:22
  186.4 0.9 copy-start.29
  187.4 1.9 copy-start.1
  187.4 1.1 copy-start.4
  187.4 1.2 copy-start.5
  199.2 18.1 %all-to-all-start.13 = ((f32[64,1,1024]{2,1,0:T(1,128)}), f32[64,1,1024]{2,1,0:T(1,128)S(1)}, u32[]{:S(2)}, u32[]{:S(2)}) async-start(f32[64,1,1024]{2,1,0:T(1,128)} %reshape.439), calls=%async_computation.13 | async-start | bytes 524288 | tf_op jit(solution)/shard_map/all_to_all | solution.py:106
  (10 other events, 6.8 us)
where the time goes:
time: 222 us; the launch traced here: 220 us
  waiting for transfers between devices  88.5 us (40%)
  starting transfers between devices  60.7 us (27%)
  local copies, waits for them, and re-layouts  29 us (13%)
  blocking collectives  26.2 us (12%)
  other arithmetic  8.99 us (4%)
  matrix products  5.3 us (2%)
    all_to_all x4, waiting for transfers between devices, from_everyone(): lax.all_to_all(jnp.broadcast_to(value[None], (length, *value.shape)), axi...  30.2 us
    all_to_all x4, starting transfers between devices, from_everyone(): lax.all_to_all(jnp.broadcast_to(value[None], (length, *value.shape)), axi...  30 us
    unnamed x84, local copies, waits for them, and re-layouts  18.1 us
    all_to_all x2, blocking collectives, from_everyone(): lax.all_to_all(jnp.broadcast_to(value[None], (length, *value.shape)), axi...  13.9 us
    all_to_all x1, waiting for transfers between devices, summed_rows(): lax.all_to_all(nearer, far, split_axis=0, concat_axis=0, tiled=True)  13.4 us
    all_to_all x1, waiting for transfers between devices, sum_in_two_steps(): lax.all_to_all(own.astype(jnp.bfloat16), far, 0, 0, tiled=True)  11.9 us
    all_to_all x1, waiting for transfers between devices, shards(): lax.all_to_all(input_part, KV, split_axis=0, concat_axis=1, tiled=True)  10.1 us
    all_to_all x1, waiting for transfers between devices, shards(): by_head = lax.all_to_all(gated, KV, split_axis=1, concat_axis=0, tiled=True)  10.1 us
  transfers between devices with their start and end apart: 10, of which 9 were waited for; matrix products, arithmetic and copies ran while one was open for 6% of the time, Pallas kernels for 0%

commit v1 on v0

v1 whole, which is shorter than its diff:
```python
import jax
import jax.numpy as jnp
from jax import lax
from jax.experimental import pallas as pl
from jax.experimental.pallas import tpu as pltpu
from jax.sharding import PartitionSpec as P

F32 = jnp.float32
BF16 = jnp.bfloat16
MESH = pl.DeviceIdType.MESH
EPS = 1e-05
N = 64
DP_KV = ("dp", "kv")
KV_TP = ("kv", "tp")
NAMES = (
    "hid",
    "mg",
    "gate",
    "inner",
    "inp",
    "outp",
    "stepw",
    "bias",
    "dlog",
    "skip",
    "tinner",
    "tin",
    "tout",
    "rinner",
    "rin",
    "rout",
    "states",
    "binner",
    "binput",
    "bdecay",
    "lens",
    "normg",
    "mo",
    "cg",
    "eg",
    "ev",
    "rp",
)


def silu(v):
    return v / (1.0 + jnp.exp(-v))


def iota(shape, dim):
    return lax.broadcasted_iota(jnp.int32, shape, dim)


def dot(a, b):
    return jnp.dot(a, b, preferred_element_type=F32)


def dot_t(a, b):
    return lax.dot_general(a, b, (((1,), (1,)), ((), ())), preferred_element_type=F32)


def far(i):
    return lax.rem(4 + jnp.where(lax.rem(i, 2) == 1, -((i + 1) // 2), i // 2) + 8, 8)


def peer(me, i):
    return lax.rem(me // 8 + far(i // 8), 8) * 8 + lax.rem(lax.rem(me, 8) + far(lax.rem(i, 8)), 8)


def halves(x):
    return jnp.concatenate([x[:8, :], x[8:, :]], axis=1)


def diagonal(d, mask):
    return jnp.sum(jnp.where(mask, d.reshape(64, 32, 64), 0.0), axis=0)


def kernel(*refs):
    names = NAMES
    h = dict(zip(names, refs))
    out_ref = refs[len(names)]
    local = [n for n in names if n not in ("lens", "mo", "eg", "ev", "rp")]
    rest = refs[len(names) + 1 :]
    v = dict(zip(local, rest))
    (
        wproj, moF, egF, evF, rpF, we, wt, rt, rpt, cio, cpi, msuf, s2,
        srcA, bufA, msgB, recvB, msgC, recvC, pairC, msgD, recvD, srcE, bufE, msgF, recvF,
        lsem, csem, xs, xr, ss, rs, ps, pr,
    ) = rest[len(local) :]
    me, tp = lax.axis_index("kv"), lax.axis_index("tp")
    first = tp == 0

    barrier = pltpu.get_barrier_semaphore()

    def greet(o, c):
        pl.semaphore_signal(
            barrier, inc=1, device_id={"kv": lax.rem(me + o, N)}, device_id_type=MESH
        )
        return c

    pl.semaphore_signal(barrier, inc=1, device_id={"tp": 1 - tp}, device_id_type=MESH)
    lax.fori_loop(1, N, greet, 0)

    loads = {n: pltpu.make_async_copy(h[n], v[n], lsem.at[i]) for i, n in enumerate(local)}
    shared = (("mo", moF), ("eg", egF), ("ev", evF), ("rp", rpF))
    mine = [pltpu.make_async_copy(h[n], f.at[tp], csem.at[i]) for i, (n, f) in enumerate(shared)]
    for c in loads.values():
        c.start()
    for c in mine:
        c.start()

    def send_all(p, source, target):
        def one(i, c):
            t = peer(me, i)
            pltpu.make_async_remote_copy(
                src_ref=source(t),
                dst_ref=target.at[me],
                send_sem=ss.at[p],
                recv_sem=rs.at[p],
                device_id={"kv": t},
                device_id_type=MESH,
            ).start()
            return c

        lax.fori_loop(0, N - 1, one, 0)

    def all_of(sem, buf):
        most = buf.at[pl.ds(0, N - 1)]
        pltpu.make_async_copy(most, most, sem).wait()

    def swap(p, source, target):
        return pltpu.make_async_remote_copy(
            src_ref=source,
            dst_ref=target,
            send_sem=ps.at[p],
            recv_sem=pr.at[p],
            device_id={"tp": 1 - tp},
            device_id_type=MESH,
        )

    for c in loads.values():
        c.wait()
    x_own = halves(v["hid"][...].astype(F32))
    srcA[...] = x_own.astype(BF16)
    bufA[tp, me] = x_own.astype(BF16)

    gain = v["mg"][...]
    wproj[0:32] = (v["gate"][...].astype(F32) * gain).astype(BF16)
    wproj[32:64] = (v["inner"][...].astype(F32) * gain).astype(BF16)
    wproj[64:80] = (v["inp"][...].astype(F32) * gain).astype(BF16)
    wproj[80:96] = (v["outp"][...].astype(F32) * gain).astype(BF16)
    wproj[96:128] = jnp.zeros((32, 2048), BF16)
    wproj[128:192] = (v["stepw"][...].astype(F32) * gain).astype(BF16)

    for a, (t, r) in enumerate((("tout", "rout"), ("tin", "rin"))):
        taps, rec = v[t][...], v[r][...].astype(F32)
        past = jnp.sum(rec * taps[:3], axis=0, keepdims=True)
        for g in range(8):
            at = slice(g * 128, (g + 1) * 128)
            cio[2 * a, g * 8 : (g + 1) * 8] = jnp.broadcast_to(past[:, at], (8, 128))
            cio[2 * a + 1, g * 8 : (g + 1) * 8] = jnp.broadcast_to(taps[3:4, at], (8, 128))
    taps, rec = v["tinner"], v["rinner"]
    cpi[...] = (
        taps[0] * rec[0].astype(F32) + taps[1] * rec[1].astype(F32) + taps[2] * rec[2].astype(F32)
    )

    live = (iota((64, 128), 1) < h["lens"][0]).astype(F32)
    masked = v["bdecay"][...] * live
    later = (iota((128, 128), 0) > iota((128, 128), 1)).astype(F32)
    msuf[...] = jnp.dot(
        masked, later, preferred_element_type=F32, precision=lax.Precision.HIGHEST
    )
    diag = iota((64, 64), 0) == iota((64, 64), 1)
    cached = jnp.sum(masked, axis=1, keepdims=True)
    cached_row = jnp.sum(jnp.where(diag, cached, 0.0), axis=0, keepdims=True)
    whole = v["states"][...]
    high = whole.astype(BF16)
    s2[:, 0:128] = high
    s2[:, 128:256] = (whole - high.astype(F32)).astype(BF16)

    pl.semaphore_wait(barrier, N)

    send_all(0, lambda t: srcA, bufA.at[tp])
    swaps = [
        pltpu.make_async_remote_copy(
            src_ref=h[n],
            dst_ref=f.at[tp],
            send_sem=xs.at[i],
            recv_sem=xr.at[i],
            device_id={"tp": 1 - tp},
            device_id_type=MESH,
        )
        for i, (n, f) in enumerate(shared)
    ]
    for c in swaps:
        c.start()
    for c in mine:
        c.wait()
    for c in swaps:
        c.wait()

    def own_rows(x):
        x = x.reshape(64, 2, 16, x.shape[-1])
        x = jnp.where(first, x[:, 0], x[:, 1])
        return x[:, :8].reshape(512, -1), x[:, 8:].reshape(512, -1)

    low, up = own_rows(
        jnp.concatenate([moF[0].astype(F32), moF[1].astype(F32)], axis=0).T
    )
    wt[...] = jnp.concatenate([low, up], axis=1).astype(BF16)
    gain2 = v["cg"][...]
    we[...] = jnp.zeros((192, 2048), BF16)
    rpt[...] = jnp.zeros((128, 2048), F32)
    for t in range(2):
        we[t * 48 : t * 48 + 44] = (egF[t].astype(F32) * gain2).astype(BF16)
        we[96 + t * 48 : 96 + t * 48 + 44] = (evF[t].astype(F32) * gain2).astype(BF16)
        rpt[t * 48 : t * 48 + 44] = rpF[t].astype(F32)
    low, up = own_rows(rpt[...].T)
    rt[:, 0:128] = low.astype(BF16)
    rt[:, 128:256] = up.astype(BF16)

    def gathered(p, src, buf):
        all_of(rs.at[p], buf.at[tp])
        c = swap(p, buf.at[tp], buf.at[tp])
        c.start()
        c.wait()
        x0, x1 = buf[0].astype(F32), buf[1].astype(F32)
        squares = jnp.sum(jnp.sum(x0 * x0 + x1 * x1, axis=0), axis=0, keepdims=True)
        squares = squares[:, 0:64] + squares[:, 64:128]
        rms = lax.rsqrt(squares / 2048.0 + EPS)
        full = jnp.concatenate(
            [x0[:, :, 0:64], x0[:, :, 64:128], x1[:, :, 0:64], x1[:, :, 64:128]], axis=1
        )
        return full.reshape(2048, 64).astype(BF16), rms

    x, rms = gathered(0, srcA, bufA)
    u = (dot(wproj[...], x) * rms).astype(BF16).astype(F32)
    by_seq = jnp.concatenate([u, jnp.zeros((64, 64), F32)], axis=0).T
    msgB[...] = by_seq[:, 0:128].reshape(64, 1, 128)
    recvB[me] = msgB[me]
    send_all(1, lambda t: msgB.at[t], recvB)

    step_pre = jnp.sum(
        jnp.where(iota((64, 64), 0) == me, by_seq[:, 128:192], 0.0), axis=0, keepdims=True
    )
    shifted = step_pre + v["bias"][...]
    step = jnp.maximum(shifted, 0.0) + jnp.log1p(jnp.exp(-jnp.abs(shifted)))
    decay = -jnp.exp(v["dlog"][...]) * step
    e_total = jnp.exp(decay + cached_row)
    decay_col = jnp.sum(jnp.where(diag, decay, 0.0), axis=1, keepdims=True)
    faded = live * jnp.exp(decay_col + msuf[...])

    n_of, k_of = iota((128, 256), 1), iota((128, 256), 0)
    base = jnp.where(n_of < 128, 80, 64)
    spread = ((k_of - base) == (n_of & 15)).astype(BF16)
    here = ((iota((64, 256), 1) & 127) >> 4) == (iota((64, 256), 0) & 7)
    group = ((iota((64, 64), 0) >> 3) == (iota((64, 64), 1) >> 3)).astype(BF16)
    own_head = iota((64, 32, 64), 0) == iota((64, 32, 64), 2)

    all_of(rs.at[1], recvB)
    heads = recvB[...].reshape(64, 128)
    placed = jnp.where(here, dot(heads.astype(BF16), spread), 0.0).astype(BF16)
    maps = dot(group, placed)
    readout = silu(cio[0] + cio[1] * maps[:, 0:128]).astype(BF16)
    conv_input = silu(cio[2] + cio[3] * maps[:, 128:256])
    readout_f = readout.astype(F32)
    own_score = jnp.sum(readout_f * conv_input, axis=1, keepdims=True)
    own_row = jnp.sum(jnp.where(diag, own_score, 0.0), axis=0, keepdims=True)
    of_group = iota((64, 128), 0) >> 3
    blocks = jnp.concatenate(
        [jnp.where(of_group == g, readout_f, 0.0) for g in range(8)], axis=1
    ).astype(BF16)
    score = dot_t(blocks, v["binput"][...])
    weight = (faded * score).astype(BF16)
    from_block = diagonal(dot_t(v["binner"][...], weight), own_head)
    twice = jnp.concatenate([readout, readout], axis=1)
    from_state = diagonal(dot_t(s2[...], twice), own_head)
    by_channel = heads.T
    conv_inner = silu(cpi[...] + v["tinner"][3] * by_channel[32:64])
    mix = from_block + e_total * from_state + (own_row * step + v["skip"][...]) * conv_inner
    raw = mix * silu(by_channel[0:32])
    squares = jnp.sum(jnp.sum(raw * raw, axis=1, keepdims=True), axis=0, keepdims=True)
    gated = (raw * v["normg"][...]).astype(BF16).astype(F32)
    out_c = jnp.concatenate(
        [
            jnp.where(first, gated, 0.0),
            jnp.where(first, 0.0, gated),
            jnp.where(iota((8, 64), 0) == tp, squares, 0.0),
            jnp.zeros((56, 64), F32),
        ],
        axis=0,
    )
    msgC[...] = out_c.T.reshape(64, 1, 128)
    recvC[me] = msgC[me]
    send_all(2, lambda t: msgC.at[t], recvC)

    all_of(rs.at[2], recvC)
    c = swap(2, recvC, pairC)
    c.start()
    c.wait()
    g = (recvC[...] + pairC[...]).reshape(64, 128).T
    rms_gate = lax.rsqrt((g[64:65] + g[65:66]) / 4096.0 + EPS)
    zero = jnp.zeros((64, 64), F32)
    gg = jnp.concatenate(
        [jnp.concatenate([g[0:64], zero], axis=1), jnp.concatenate([zero, g[0:64]], axis=1)],
        axis=0,
    ).astype(BF16)
    rms2 = jnp.concatenate([rms_gate, rms_gate], axis=1)
    msgD[...] = (dot(wt[...], gg) * rms2).astype(BF16).reshape(64, 8, 128)
    recvD[me] = msgD[me]
    send_all(3, lambda t: msgD.at[t], recvD)
    all_of(rs.at[3], recvD)
    mid = (x_own + jnp.sum(recvD[...].astype(F32), axis=0)).astype(BF16)
    srcE[...] = mid
    bufE[tp, me] = mid
    send_all(4, lambda t: srcE, bufE.at[tp])
    y, rms = gathered(4, srcE, bufE)
    u = dot(we[...], y) * rms
    act = silu(u[0:96]) * u[96:192]
    zero = jnp.zeros((96, 64), F32)
    pad = jnp.zeros((32, 128), F32)
    aa = jnp.concatenate(
        [
            jnp.concatenate([act, zero], axis=1),
            pad,
            jnp.concatenate([zero, act], axis=1),
            pad,
        ],
        axis=0,
    ).astype(BF16)
    msgF[...] = dot(rt[...], aa).astype(BF16).reshape(64, 8, 128)
    recvF[me] = msgF[me]
    send_all(5, lambda t: msgF.at[t], recvF)
    all_of(rs.at[5], recvF)
    end = mid.astype(F32) + jnp.sum(recvF[...].astype(F32), axis=0)
    out_ref[...] = jnp.concatenate([end[:, 0:64], end[:, 64:128]], axis=0).astype(BF16)
    for p, b in ((0, bufA.at[0]), (1, recvB), (2, recvC), (3, recvD), (4, bufE.at[0]), (5, recvF)):
        all_of(ss.at[p], b)


def shards(
    hidden, mixer_gain, gate_proj, inner_proj, input_proj, output_proj, step_proj, step_bias,
    decay_log, skip_gain, taps_inner, taps_input, taps_output, recent_inner, recent_input,
    recent_output, states, block_inner, block_input, block_decay, lengths, norm_gain, mixer_out,
    channel_gain, expand_gate, expand_value, reduce_proj,
):
    args = dict(
        hid=hidden,
        mg=mixer_gain.reshape(1, 2048),
        gate=gate_proj.transpose(1, 2, 0).reshape(32, 2048),
        inner=inner_proj.transpose(1, 2, 0).reshape(32, 2048),
        inp=input_proj.T,
        outp=output_proj.T,
        stepw=step_proj.T,
        bias=step_bias.reshape(1, 64),
        dlog=decay_log.reshape(1, 64),
        skip=skip_gain.reshape(1, 64),
        tinner=taps_inner.transpose(0, 2, 1),
        tin=taps_input,
        tout=taps_output,
        rinner=recent_inner.transpose(0, 1, 3, 2).reshape(3, 32, 64),
        rin=recent_input.reshape(3, 1024),
        rout=recent_output.reshape(3, 1024),
        states=states.reshape(2048, 128),
        binner=block_inner.transpose(0, 2, 3, 1).reshape(2048, 128),
        binput=block_input.reshape(128, 1024),
        bdecay=block_decay.transpose(0, 2, 1).reshape(64, 128),
        lens=lengths,
        normg=norm_gain.T,
        mo=mixer_out.reshape(32, 2048),
        cg=channel_gain.reshape(1, 2048),
        eg=expand_gate.T,
        ev=expand_value.T,
        rp=reduce_proj,
    )
    away = ("lens", "mo", "eg", "ev", "rp")
    near = [pltpu.VMEM(a.shape, a.dtype) for n, a in args.items() if n not in away]
    scratch = near + [
        pltpu.VMEM((192, 2048), BF16),
        pltpu.VMEM((2, 32, 2048), BF16),
        pltpu.VMEM((2, 44, 2048), BF16),
        pltpu.VMEM((2, 44, 2048), BF16),
        pltpu.VMEM((2, 44, 2048), BF16),
        pltpu.VMEM((192, 2048), BF16),
        pltpu.VMEM((512, 128), BF16),
        pltpu.VMEM((512, 256), BF16),
        pltpu.VMEM((128, 2048), F32),
        pltpu.VMEM((4, 64, 128), F32),
        pltpu.VMEM((32, 64), F32),
        pltpu.VMEM((64, 128), F32),
        pltpu.VMEM((2048, 256), BF16),
        pltpu.VMEM((8, 128), BF16),
        pltpu.VMEM((2, N, 8, 128), BF16),
        pltpu.VMEM((N, 1, 128), F32),
        pltpu.VMEM((N, 1, 128), F32),
        pltpu.VMEM((N, 1, 128), F32),
        pltpu.VMEM((N, 1, 128), F32),
        pltpu.VMEM((N, 1, 128), F32),
        pltpu.VMEM((N, 8, 128), BF16),
        pltpu.VMEM((N, 8, 128), BF16),
        pltpu.VMEM((8, 128), BF16),
        pltpu.VMEM((2, N, 8, 128), BF16),
        pltpu.VMEM((N, 8, 128), BF16),
        pltpu.VMEM((N, 8, 128), BF16),
        pltpu.SemaphoreType.DMA((len(near),)),
        pltpu.SemaphoreType.DMA((4,)),
        pltpu.SemaphoreType.DMA((4,)),
        pltpu.SemaphoreType.DMA((4,)),
        pltpu.SemaphoreType.DMA((6,)),
        pltpu.SemaphoreType.DMA((6,)),
        pltpu.SemaphoreType.DMA((6,)),
        pltpu.SemaphoreType.DMA((6,)),
    ]
    space = [
        pl.BlockSpec(memory_space=pltpu.SMEM if n == "lens" else pl.ANY) for n in args
    ]
    return pl.pallas_call(
        kernel,
        out_shape=jax.ShapeDtypeStruct((16, 64), BF16),
        in_specs=space,
        out_specs=pl.BlockSpec(memory_space=pltpu.VMEM),
        scratch_shapes=scratch,
        compiler_params=pltpu.CompilerParams(collective_id=0, has_side_effects=True),
    )(*args.values())


def solution(mesh):
    in_specs = (
        P(KV_TP, "dp"),
        P(),
        P(None, "kv", "tp"),
        P(None, "kv", "tp"),
        P(None, "kv"),
        P(None, "kv"),
        P(),
        P(),
        P(),
        P(),
        P(None, None, "tp"),
        P(),
        P(),
        P(DP_KV, None, None, "tp"),
        P(DP_KV, None, None),
        P(DP_KV, None, None),
        P(DP_KV, None, "tp", None),
        P(DP_KV, None, None, "tp"),
        P(DP_KV, None, None),
        P(DP_KV, None, None),
        P(DP_KV),
        P(None, "tp"),
        P("kv", "tp", None),
        P(),
        P(None, KV_TP),
        P(None, KV_TP),
        P(KV_TP, None),
    )
    return jax.shard_map(
        shards, mesh=mesh, in_specs=in_specs, out_specs=P(KV_TP, "dp"), check_vma=False
    )
```

time: 222 us -> 71.5 us (0.32)
  waiting for transfers between devices: 88.5 us -> 0 us
  Pallas kernels: 0 us -> 69.4 us
  starting transfers between devices: 60.7 us -> 0 us
  local copies, waits for them, and re-layouts: 29 us -> 1.28 us
  blocking collectives: 26.2 us -> 0 us
  other arithmetic: 8.99 us -> 0 us
  matrix products: 5.3 us -> 0 us
    all_to_all x10 -> x0, waiting for transfers between devices: 88.5 us -> none  [the longest x4 30.2 us: from_everyone(): lax.all_to_all(jnp.broadcast_to(value[None], (length, *value.shape)), axi...]
    pallas_call x0 -> x1, Pallas kernels: none -> 69.4 us  [shards(): pl.pallas_call(kernel, out_shape=jax.ShapeDtypeStruct((16, 64), BF16), in...]
    all_to_all x10 -> x0, starting transfers between devices: 60.7 us -> none  [the longest x4 30 us: from_everyone(): lax.all_to_all(jnp.broadcast_to(value[None], (length, *value.shape)), axi...]
    all_to_all x4 -> x0, blocking collectives: 26.2 us -> none  [the longest x2 13.9 us: from_everyone(): lax.all_to_all(jnp.broadcast_to(value[None], (length, *value.shape)), axi...]
    unnamed x84 -> x1, local copies, waits for them, and re-layouts: 18.1 us -> 1.28 us
    dot_general x10 -> x0, matrix products: 5.3 us -> none  [the longest x1 2.13 us: shards(): jnp.einsum('sgn,sgrpn->sgrp', readout_f, grouped, precision=lax.Precision...]
    all_to_all x4 -> x0, other arithmetic: 3.75 us -> none  [the longest x1 2.3 us: summed_on_arrival(): lax.all_to_all(in_blocks(value, dim, length), axis, 0, 0, tiled=True)]
    reduce_sum x13 -> x0, other arithmetic: 2.67 us -> none  [the longest x1 0.68 us: shards(): cached = jnp.sum(masked, axis=1)]
  transfers between devices with their start and end apart: 10 -> 0, of which waited for: 9 -> 0; matrix products, arithmetic and copies ran while one was open for 6% -> 0% of each run, Pallas kernels for 0% -> 0%
where the time goes in v1:
time: 71.5 us; the launch traced here: 71.4 us
  Pallas kernels  69.4 us (97%)
  local copies, waits for them, and re-layouts  1.28 us (2%)
    pallas_call x1, Pallas kernels, shards(): pl.pallas_call(kernel, out_shape=jax.ShapeDtypeStruct((16, 64), BF16), in...  69.4 us

profile of v1, /device:TPU:1, one launch (start us, length us, event | category | flops | bytes accessed | tf_op | source)
XLA Modules:
  0.0 71.4 jit_solution(3356139484521259820)
XLA Ops:
  0.7 69.4 %shard_map.253 = bf16[16,64]{1,0:T(8,128)(2,1)} custom-call(bf16[16,64]{1,0:T(8,128)(2,1)} %refs_0_.1, f32[1,2048]{1,0:T(1,128)} %bitcast.47, bf16[32,2048]{1,0:T(8,128)(2,1)} %bitcast.38, bf16[32,2048]{1,0:T(8,128)(2,1)} %bitcast.39, bf16[16,2048]{1,0:T(8,128)(2,1)} %bitcast.41, bf16[16,2048]{1,0:T(8,128)(2,1)} %bitcast.42, bf16[64,2048]{1,0:T(8,128)(2,1)} %bitcast.34, ...), custom_call_target="tpu_custom_call" | custom-call | tf_op jit(solution)/shard_map/pallas_call | solution.py:417
  70.1 1.3 %copy.30 = bf16[16,64]{1,0:T(8,128)(2,1)} copy(bf16[16,64]{1,0:T(8,128)(2,1)} %shard_map.253) | data formatting | bytes 4096

commit v2 on v1

--- a/solution.py
+++ b/solution.py
@@ -79,12 +79,12 @@
     names = NAMES
     h = dict(zip(names, refs))
     out_ref = refs[len(names)]
-    local = [n for n in names if n not in ("lens", "mo", "eg", "ev", "rp")]
+    local = [n for n in names if n not in ("eg", "ev", "rp")]
     rest = refs[len(names) + 1 :]
     v = dict(zip(local, rest))
     (
-        wproj, moF, egF, evF, rpF, we, wt, rt, rpt, cio, cpi, msuf, s2,
-        srcA, bufA, msgB, recvB, msgC, recvC, pairC, msgD, recvD, srcE, bufE, msgF, recvF,
+        wproj, egF, evF, rpF, we, wd, rt, rpt, cio, cpi, msuf, s2, gf,
+        srcA, bufA, msgB, recvB, srcC, recvC, sumC, pairC, msgW, recvW, srcE, bufE, msgF, recvF,
         lsem, csem, xs, xr, ss, rs, ps, pr,
     ) = rest[len(local) :]
     me, tp = lax.axis_index("kv"), lax.axis_index("tp")
@@ -102,7 +102,7 @@
     lax.fori_loop(1, N, greet, 0)
 
     loads = {n: pltpu.make_async_copy(h[n], v[n], lsem.at[i]) for i, n in enumerate(local)}
-    shared = (("mo", moF), ("eg", egF), ("ev", evF), ("rp", rpF))
+    shared = (("eg", egF), ("ev", evF), ("rp", rpF))
     mine = [pltpu.make_async_copy(h[n], f.at[tp], csem.at[i]) for i, (n, f) in enumerate(shared)]
     for c in loads.values():
         c.start()
@@ -164,7 +164,7 @@
         taps[0] * rec[0].astype(F32) + taps[1] * rec[1].astype(F32) + taps[2] * rec[2].astype(F32)
     )
 
-    live = (iota((64, 128), 1) < h["lens"][0]).astype(F32)
+    live = (iota((64, 128), 1) < v["lens"][0:1, 0:1]).astype(F32)
     masked = v["bdecay"][...] * live
     later = (iota((128, 128), 0) > iota((128, 128), 1)).astype(F32)
     msuf[...] = jnp.dot(
@@ -177,6 +177,16 @@
     high = whole.astype(BF16)
     s2[:, 0:128] = high
     s2[:, 128:256] = (whole - high.astype(F32)).astype(BF16)
+
+    lane = iota((32, 64), 1)
+    norm = jnp.sum(jnp.where(lane == me, v["normg"][...], 0.0), axis=1, keepdims=True)
+    rows = jnp.concatenate([v["mo"][...].astype(F32) * norm, jnp.zeros((96, 2048), F32)], axis=0)
+    rows = rows.T.reshape(64, 4, 8, 128)
+    packed = rows[:, 0].reshape(512, 128)
+    for q in range(1, 4):
+        packed = packed + pltpu.roll(rows[:, q].reshape(512, 128), 32 * q, 1)
+    msgW[...] = packed.astype(BF16).reshape(64, 8, 128)
+    recvW[me] = msgW[me]
 
     pl.semaphore_wait(barrier, N)
 
@@ -204,10 +214,6 @@
         x = jnp.where(first, x[:, 0], x[:, 1])
         return x[:, :8].reshape(512, -1), x[:, 8:].reshape(512, -1)
 
-    low, up = own_rows(
-        jnp.concatenate([moF[0].astype(F32), moF[1].astype(F32)], axis=0).T
-    )
-    wt[...] = jnp.concatenate([low, up], axis=1).astype(BF16)
     gain2 = v["cg"][...]
     we[...] = jnp.zeros((192, 2048), BF16)
     rpt[...] = jnp.zeros((128, 2048), F32)
@@ -239,6 +245,7 @@
     msgB[...] = by_seq[:, 0:128].reshape(64, 1, 128)
     recvB[me] = msgB[me]
     send_all(1, lambda t: msgB.at[t], recvB)
+    send_all(3, lambda t: msgW.at[t], recvW)
 
     step_pre = jnp.sum(
         jnp.where(iota((64, 64), 0) == me, by_seq[:, 128:192], 0.0), axis=0, keepdims=True
@@ -279,38 +286,45 @@
     conv_inner = silu(cpi[...] + v["tinner"][3] * by_channel[32:64])
     mix = from_block + e_total * from_state + (own_row * step + v["skip"][...]) * conv_inner
     raw = mix * silu(by_channel[0:32])
-    squares = jnp.sum(jnp.sum(raw * raw, axis=1, keepdims=True), axis=0, keepdims=True)
-    gated = (raw * v["normg"][...]).astype(BF16).astype(F32)
-    out_c = jnp.concatenate(
-        [
-            jnp.where(first, gated, 0.0),
-            jnp.where(first, 0.0, gated),
-            jnp.where(iota((8, 64), 0) == tp, squares, 0.0),
-            jnp.zeros((56, 64), F32),
-        ],
-        axis=0,
-    )
-    msgC[...] = out_c.T.reshape(64, 1, 128)
-    recvC[me] = msgC[me]
-    send_all(2, lambda t: msgC.at[t], recvC)
+    by_head = jnp.concatenate([raw, jnp.zeros((96, 64), F32)], axis=0).T
+    packed = by_head[0:16]
+    for q in range(1, 4):
+        packed = packed + pltpu.roll(by_head[q * 16 : (q + 1) * 16], 32 * q, 1)
+    srcC[...] = packed.astype(BF16)
+    recvC[me] = packed.astype(BF16)
+    send_all(2, lambda t: srcC, recvC)
+
+    all_of(rs.at[3], recvW)
+    tiles = recvW[...].astype(F32).reshape(4, 128, 128)
+    block = iota((128, 128), 1) >> 5
+    for dd in range(4):
+        out = jnp.zeros((128, 128), F32)
+        for q in range(4):
+            turned = tiles[q] if q == dd else pltpu.roll(tiles[q], (32 * (q - dd)) % 128, 1)
+            out = jnp.where(block == q, turned, out)
+        out = out.astype(BF16).reshape(16, 8, 128)
+        for i in range(16):
+            wd[i // 2, dd * 8 : dd * 8 + 8, (i % 2) * 128 : (i % 2) * 128 + 128] = out[i]
 
     all_of(rs.at[2], recvC)
-    c = swap(2, recvC, pairC)
+    gates = recvC[...].astype(F32)
+    gf[...] = gates.reshape(1024, 128)
+    partial = jnp.zeros((32, 64), F32)
+    for i in range(8):
+        pair = [gf[pl.ds(2 * i + e, 64, stride=16), :] for e in range(2)]
+        partial = partial + dot_t(wd[i], jnp.concatenate(pair, axis=1).astype(BF16))
+    squares = jnp.sum(jnp.sum(gates * gates, axis=1), axis=1, keepdims=True)
+    squares = jnp.sum(jnp.where(diag, squares, 0.0), axis=0, keepdims=True)
+    squares = jnp.broadcast_to(jnp.concatenate([squares, squares], axis=1), (8, 128))
+    part0, part1 = halves(partial[0:16]), halves(partial[16:32])
+    sumC[0:8] = jnp.where(first, part1, part0)
+    sumC[8:16] = squares
+    c = swap(2, sumC, pairC)
     c.start()
     c.wait()
-    g = (recvC[...] + pairC[...]).reshape(64, 128).T
-    rms_gate = lax.rsqrt((g[64:65] + g[65:66]) / 4096.0 + EPS)
-    zero = jnp.zeros((64, 64), F32)
-    gg = jnp.concatenate(
-        [jnp.concatenate([g[0:64], zero], axis=1), jnp.concatenate([zero, g[0:64]], axis=1)],
-        axis=0,
-    ).astype(BF16)
-    rms2 = jnp.concatenate([rms_gate, rms_gate], axis=1)
-    msgD[...] = (dot(wt[...], gg) * rms2).astype(BF16).reshape(64, 8, 128)
-    recvD[me] = msgD[me]
-    send_all(3, lambda t: msgD.at[t], recvD)
-    all_of(rs.at[3], recvD)
-    mid = (x_own + jnp.sum(recvD[...].astype(F32), axis=0)).astype(BF16)
+    mixed = jnp.where(first, part0, part1) + pairC[0:8]
+    mixed = mixed * lax.rsqrt((squares + pairC[8:16]) / 4096.0 + EPS)
+    mid = (x_own + mixed).astype(BF16)
     srcE[...] = mid
     bufE[tp, me] = mid
     send_all(4, lambda t: srcE, bufE.at[tp])
@@ -333,8 +347,8 @@
     send_all(5, lambda t: msgF.at[t], recvF)
     all_of(rs.at[5], recvF)
     end = mid.astype(F32) + jnp.sum(recvF[...].astype(F32), axis=0)
-    out_ref[...] = jnp.concatenate([end[:, 0:64], end[:, 64:128]], axis=0).astype(BF16)
-    for p, b in ((0, bufA.at[0]), (1, recvB), (2, recvC), (3, recvD), (4, bufE.at[0]), (5, recvF)):
+    out_ref[...] = jnp.concatenate([end[:, 0:64], end[:, 64:128]], axis=0)
+    for p, b in ((0, bufA.at[0]), (1, recvB), (2, recvC), (3, recvW), (4, bufE.at[0]), (5, recvF)):
         all_of(ss.at[p], b)
 
 
@@ -365,7 +379,7 @@
         binner=block_inner.transpose(0, 2, 3, 1).reshape(2048, 128),
         binput=block_input.reshape(128, 1024),
         bdecay=block_decay.transpose(0, 2, 1).reshape(64, 128),
-        lens=lengths,
+        lens=lengths.reshape(1, 1),
         normg=norm_gain.T,
         mo=mixer_out.reshape(32, 2048),
         cg=channel_gain.reshape(1, 2048),
@@ -373,29 +387,34 @@
         ev=expand_value.T,
         rp=reduce_proj,
     )
-    away = ("lens", "mo", "eg", "ev", "rp")
-    near = [pltpu.VMEM(a.shape, a.dtype) for n, a in args.items() if n not in away]
+    away = ("eg", "ev", "rp")
+    near = [
+        pltpu.VMEM(a.shape, a.dtype)
+        for n, a in args.items()
+        if n not in away
+    ]
     scratch = near + [
         pltpu.VMEM((192, 2048), BF16),
-        pltpu.VMEM((2, 32, 2048), BF16),
         pltpu.VMEM((2, 44, 2048), BF16),
         pltpu.VMEM((2, 44, 2048), BF16),
         pltpu.VMEM((2, 44, 2048), BF16),
         pltpu.VMEM((192, 2048), BF16),
-        pltpu.VMEM((512, 128), BF16),
+        pltpu.VMEM((8, 32, 256), BF16),
         pltpu.VMEM((512, 256), BF16),
         pltpu.VMEM((128, 2048), F32),
         pltpu.VMEM((4, 64, 128), F32),
         pltpu.VMEM((32, 64), F32),
         pltpu.VMEM((64, 128), F32),
         pltpu.VMEM((2048, 256), BF16),
+        pltpu.VMEM((1024, 128), F32),
         pltpu.VMEM((8, 128), BF16),
         pltpu.VMEM((2, N, 8, 128), BF16),
         pltpu.VMEM((N, 1, 128), F32),
         pltpu.VMEM((N, 1, 128), F32),
-        pltpu.VMEM((N, 1, 128), F32),
-        pltpu.VMEM((N, 1, 128), F32),
-        pltpu.VMEM((N, 1, 128), F32),
+        pltpu.VMEM((16, 128), BF16),
+        pltpu.VMEM((N, 16, 128), BF16),
+        pltpu.VMEM((16, 128), F32),
+        pltpu.VMEM((16, 128), F32),
         pltpu.VMEM((N, 8, 128), BF16),
         pltpu.VMEM((N, 8, 128), BF16),
         pltpu.VMEM((8, 128), BF16),
@@ -403,25 +422,26 @@
         pltpu.VMEM((N, 8, 128), BF16),
         pltpu.VMEM((N, 8, 128), BF16),
         pltpu.SemaphoreType.DMA((len(near),)),
-        pltpu.SemaphoreType.DMA((4,)),
-        pltpu.SemaphoreType.DMA((4,)),
-        pltpu.SemaphoreType.DMA((4,)),
+        pltpu.SemaphoreType.DMA((3,)),
+        pltpu.SemaphoreType.DMA((3,)),
+        pltpu.SemaphoreType.DMA((3,)),
         pltpu.SemaphoreType.DMA((6,)),
         pltpu.SemaphoreType.DMA((6,)),
         pltpu.SemaphoreType.DMA((6,)),
         pltpu.SemaphoreType.DMA((6,)),
     ]
     space = [
-        pl.BlockSpec(memory_space=pltpu.SMEM if n == "lens" else pl.ANY) for n in args
+        pl.BlockSpec(memory_space=pltpu.HBM if n == "lens" else pl.ANY) for n in args
     ]
-    return pl.pallas_call(
+    end = pl.pallas_call(
         kernel,
-        out_shape=jax.ShapeDtypeStruct((16, 64), BF16),
+        out_shape=pltpu.VMEM((16, 64), F32),
         in_specs=space,
         out_specs=pl.BlockSpec(memory_space=pltpu.VMEM),
         scratch_shapes=scratch,
         compiler_params=pltpu.CompilerParams(collective_id=0, has_side_effects=True),
     )(*args.values())
+    return end.astype(BF16)
 
 
 def solution(mesh):

time: 71.5 us -> 63.9 us (0.89)
  Pallas kernels: 69.4 us -> 62.5 us
  local copies, waits for them, and re-layouts: 1.28 us -> 0 us
    pallas_call x1, Pallas kernels: 69.4 us -> 62.5 us  [shards(): pl.pallas_call(kernel, out_shape=pltpu.VMEM((16, 64), F32), in_specs=spac...]
    unnamed x1 -> x0, local copies, waits for them, and re-layouts: 1.28 us -> none
where the time goes in v2:
time: 63.9 us; the launch traced here: 63.8 us
  Pallas kernels  62.5 us (98%)
  between operations  0.66 us (1%)
    pallas_call x1, Pallas kernels, shards(): pl.pallas_call(kernel, out_shape=pltpu.VMEM((16, 64), F32), in_specs=spac...  62.5 us

profile of v2, /device:TPU:1, one launch (start us, length us, event | category | flops | bytes accessed | tf_op | source)
XLA Modules:
  0.0 63.8 jit_solution(16602662223494912304)
XLA Ops:
  0.7 62.5 %shard_map.253 = f32[16,64]{1,0:T(8,128)S(1)} custom-call(bf16[16,64]{1,0:T(8,128)(2,1)} %refs_0_.1, f32[1,2048]{1,0:T(1,128)} %bitcast.49, bf16[32,2048]{1,0:T(8,128)(2,1)} %bitcast.40, bf16[32,2048]{1,0:T(8,128)(2,1)} %bitcast.41, bf16[16,2048]{1,0:T(8,128)(2,1)} %bitcast.43, bf16[16,2048]{1,0:T(8,128)(2,1)} %bitcast.44, bf16[64,2048]{1,0:T(8,128)(2,1)} %bitcast.36, ...), custom_call_target="tpu_custom_call" | custom-call | tf_op jit(solution)/shard_map/pallas_call | solution.py:436
  63.2 0.6 convert_element_type.3

commit v3 on v2

--- a/solution.py
+++ b/solution.py
@@ -59,14 +59,6 @@
     return lax.dot_general(a, b, (((1,), (1,)), ((), ())), preferred_element_type=F32)
 
 
-def far(i):
-    return lax.rem(4 + jnp.where(lax.rem(i, 2) == 1, -((i + 1) // 2), i // 2) + 8, 8)
-
-
-def peer(me, i):
-    return lax.rem(me // 8 + far(i // 8), 8) * 8 + lax.rem(lax.rem(me, 8) + far(lax.rem(i, 8)), 8)
-
-
 def halves(x):
     return jnp.concatenate([x[:8, :], x[8:, :]], axis=1)
 
@@ -79,31 +71,40 @@
     names = NAMES
     h = dict(zip(names, refs))
     out_ref = refs[len(names)]
-    local = [n for n in names if n not in ("eg", "ev", "rp")]
+    local = [n for n in names if n not in ("gate", "inner", "eg", "ev", "rp")]
     rest = refs[len(names) + 1 :]
     v = dict(zip(local, rest))
     (
-        wproj, egF, evF, rpF, we, wd, rt, rpt, cio, cpi, msuf, s2, gf,
-        srcA, bufA, msgB, recvB, srcC, recvC, sumC, pairC, msgW, recvW, srcE, bufE, msgF, recvF,
+        wfull, wproj, giF, egF, evF, rpF, we, we2, wd, rt, rpt, cio, cpi, msuf, s2, gf,
+        srcA, bufA, msgB, recvB, sumA, pairA, sumE, pairE, srcC, recvC, sumC, pairC, msgW, recvW, srcE, bufE, msgF, recvF,
         lsem, csem, xs, xr, ss, rs, ps, pr,
     ) = rest[len(local) :]
     me, tp = lax.axis_index("kv"), lax.axis_index("tp")
     first = tp == 0
 
+    order = (4, 3, 5, 2, 6, 1, 7, 0)
+    in_rows = [lax.rem(me // 8 + o, 8) * 8 for o in order]
+    in_cols = [lax.rem(lax.rem(me, 8) + o, 8) for o in order]
+    peers = [r + c for r in in_rows for c in in_cols][: N - 1]
+    dist = [min(o, 8 - o) for o in order]
+    ranks = sorted(range(N - 1), key=lambda i: -(dist[i // 8] + dist[i % 8]))
+    peers = [peers[i] for i in ranks]
+
     barrier = pltpu.get_barrier_semaphore()
 
-    def greet(o, c):
-        pl.semaphore_signal(
-            barrier, inc=1, device_id={"kv": lax.rem(me + o, N)}, device_id_type=MESH
-        )
-        return c
-
     pl.semaphore_signal(barrier, inc=1, device_id={"tp": 1 - tp}, device_id_type=MESH)
-    lax.fori_loop(1, N, greet, 0)
+    for t in peers:
+        pl.semaphore_signal(barrier, inc=1, device_id={"kv": t}, device_id_type=MESH)
 
     loads = {n: pltpu.make_async_copy(h[n], v[n], lsem.at[i]) for i, n in enumerate(local)}
-    shared = (("eg", egF), ("ev", evF), ("rp", rpF))
-    mine = [pltpu.make_async_copy(h[n], f.at[tp], csem.at[i]) for i, (n, f) in enumerate(shared)]
+    shared = (
+        ("gate", giF.at[tp, pl.ds(0, 32)]),
+        ("inner", giF.at[tp, pl.ds(32, 32)]),
+        ("eg", egF.at[tp]),
+        ("ev", evF.at[tp]),
+        ("rp", rpF.at[tp]),
+    )
+    mine = [pltpu.make_async_copy(h[n], f, csem.at[i]) for i, (n, f) in enumerate(shared)]
     for c in loads.values():
         c.start()
     for c in mine:
@@ -111,7 +112,7 @@
 
     def send_all(p, source, target):
         def one(i, c):
-            t = peer(me, i)
+            t = i
             pltpu.make_async_remote_copy(
                 src_ref=source(t),
                 dst_ref=target.at[me],
@@ -122,7 +123,8 @@
             ).start()
             return c
 
-        lax.fori_loop(0, N - 1, one, 0)
+        for t in peers:
+            one(t, 0)
 
     def all_of(sem, buf):
         most = buf.at[pl.ds(0, N - 1)]
@@ -138,19 +140,53 @@
             device_id_type=MESH,
         )
 
-    for c in loads.values():
-        c.wait()
+    loads["hid"].wait()
     x_own = halves(v["hid"][...].astype(F32))
     srcA[...] = x_own.astype(BF16)
-    bufA[tp, me] = x_own.astype(BF16)
+    bufA[me] = x_own.astype(BF16)
+    pl.semaphore_wait(barrier, N)
+
+    send_all(0, lambda t: srcA, bufA)
+    swaps = [
+        pltpu.make_async_remote_copy(
+            src_ref=h[n],
+            dst_ref=f,
+            send_sem=xs.at[i],
+            recv_sem=xr.at[i],
+            device_id={"tp": 1 - tp},
+            device_id_type=MESH,
+        )
+        for i, (n, f) in enumerate(shared)
+    ]
+    for c in swaps:
+        c.start()
+    for n in local:
+        if n != "hid":
+            loads[n].wait()
 
     gain = v["mg"][...]
-    wproj[0:32] = (v["gate"][...].astype(F32) * gain).astype(BF16)
-    wproj[32:64] = (v["inner"][...].astype(F32) * gain).astype(BF16)
-    wproj[64:80] = (v["inp"][...].astype(F32) * gain).astype(BF16)
-    wproj[80:96] = (v["outp"][...].astype(F32) * gain).astype(BF16)
-    wproj[96:128] = jnp.zeros((32, 2048), BF16)
-    wproj[128:192] = (v["stepw"][...].astype(F32) * gain).astype(BF16)
+    wfull[128:144] = (v["inp"][...].astype(F32) * gain).astype(BF16)
+    wfull[144:160] = (v["outp"][...].astype(F32) * gain).astype(BF16)
+    wfull[160:224] = (v["stepw"][...].astype(F32) * gain).astype(BF16)
+    low_lanes = iota((1, 128), 1) < 64
+    to, at = iota((512, 256), 0), iota((512, 256), 1)
+    spot = ((at & 127) >> 3) * 32 + 16 * tp + (at >> 7) * 8 + (at & 7)
+    picked = (to == spot).astype(BF16)
+
+    def pick(whole, out):
+        n = whole.shape[0]
+        for i in range(4):
+            y = dot(whole[:, i * 512 : (i + 1) * 512], picked).astype(BF16)
+            out[0:n, i * 128 : (i + 1) * 128] = y[:, 0:128]
+            out[n : 2 * n, i * 128 : (i + 1) * 128] = y[:, 128:256]
+
+    for c in mine[:2]:
+        c.wait()
+    for c in swaps[:2]:
+        c.wait()
+    for t in range(2):
+        wfull[t * 64 : t * 64 + 64] = (giF[t].astype(F32) * gain).astype(BF16)
+    pick(wfull, wproj)
 
     for a, (t, r) in enumerate((("tout", "rout"), ("tin", "rin"))):
         taps, rec = v[t][...], v[r][...].astype(F32)
@@ -188,68 +224,74 @@
     msgW[...] = packed.astype(BF16).reshape(64, 8, 128)
     recvW[me] = msgW[me]
 
-    pl.semaphore_wait(barrier, N)
-
-    send_all(0, lambda t: srcA, bufA.at[tp])
-    swaps = [
-        pltpu.make_async_remote_copy(
-            src_ref=h[n],
-            dst_ref=f.at[tp],
-            send_sem=xs.at[i],
-            recv_sem=xr.at[i],
-            device_id={"tp": 1 - tp},
-            device_id_type=MESH,
-        )
-        for i, (n, f) in enumerate(shared)
-    ]
-    for c in swaps:
-        c.start()
-    for c in mine:
-        c.wait()
-    for c in swaps:
-        c.wait()
-
     def own_rows(x):
         x = x.reshape(64, 2, 16, x.shape[-1])
         x = jnp.where(first, x[:, 0], x[:, 1])
         return x[:, :8].reshape(512, -1), x[:, 8:].reshape(512, -1)
 
-    gain2 = v["cg"][...]
-    we[...] = jnp.zeros((192, 2048), BF16)
-    rpt[...] = jnp.zeros((128, 2048), F32)
-    for t in range(2):
-        we[t * 48 : t * 48 + 44] = (egF[t].astype(F32) * gain2).astype(BF16)
-        we[96 + t * 48 : 96 + t * 48 + 44] = (evF[t].astype(F32) * gain2).astype(BF16)
-        rpt[t * 48 : t * 48 + 44] = rpF[t].astype(F32)
-    low, up = own_rows(rpt[...].T)
-    rt[:, 0:128] = low.astype(BF16)
-    rt[:, 128:256] = up.astype(BF16)
-
-    def gathered(p, src, buf):
-        all_of(rs.at[p], buf.at[tp])
-        c = swap(p, buf.at[tp], buf.at[tp])
+    def gathered(p, buf, w):
+        all_of(rs.at[p], buf)
+        x = buf[...].astype(F32)
+        squares = jnp.sum(jnp.sum(x * x, axis=0), axis=0, keepdims=True)
+        squares = squares + pltpu.roll(squares, 64, 1)
+        return dot(w[...], x.reshape(512, 128).astype(BF16)), squares
+
+    def joined(p, own, other, squares, source, target):
+        source[0:96] = other
+        source[96:104] = jnp.broadcast_to(squares, (8, 128))
+        c = swap(p, source, target)
         c.start()
         c.wait()
-        x0, x1 = buf[0].astype(F32), buf[1].astype(F32)
-        squares = jnp.sum(jnp.sum(x0 * x0 + x1 * x1, axis=0), axis=0, keepdims=True)
-        squares = squares[:, 0:64] + squares[:, 64:128]
-        rms = lax.rsqrt(squares / 2048.0 + EPS)
-        full = jnp.concatenate(
-            [x0[:, :, 0:64], x0[:, :, 64:128], x1[:, :, 0:64], x1[:, :, 64:128]], axis=1
-        )
-        return full.reshape(2048, 64).astype(BF16), rms
-
-    x, rms = gathered(0, srcA, bufA)
-    u = (dot(wproj[...], x) * rms).astype(BF16).astype(F32)
-    by_seq = jnp.concatenate([u, jnp.zeros((64, 64), F32)], axis=0).T
-    msgB[...] = by_seq[:, 0:128].reshape(64, 1, 128)
-    recvB[me] = msgB[me]
-    send_all(1, lambda t: msgB.at[t], recvB)
+        squares = squares + target[96:97]
+        return (own + target[0:96]) * lax.rsqrt(squares / 2048.0 + EPS)
+
+    u, squares = gathered(0, bufA, wproj)
+    u = u[0:224] + pltpu.roll(u[224:448], 64, 1)
+    tail = jnp.concatenate(
+        [u[128:160], jnp.broadcast_to(squares, (8, 128)), jnp.zeros((24, 128), F32)], axis=0
+    )
+    by_core = [jnp.concatenate([u[t * 64 : t * 64 + 64], tail], axis=0) for t in range(2)]
+    by_seq = jnp.where(low_lanes, by_core[0], pltpu.roll(by_core[1], 64, 1)).T
+    msgB[...] = by_seq.reshape(128, 1, 128)
+    here_b = tp * N + me
+    recvB[here_b] = msgB[here_b]
+
+    def send_parts(i, c):
+        t = i
+        for core in range(2):
+            pltpu.make_async_remote_copy(
+                src_ref=msgB.at[core * N + t],
+                dst_ref=recvB.at[here_b],
+                send_sem=ss.at[1],
+                recv_sem=rs.at[1],
+                device_id={"kv": t, "tp": core},
+                device_id_type=MESH,
+            ).start()
+        return c
+
+    for t in peers:
+        send_parts(t, 0)
+    pltpu.make_async_remote_copy(
+        src_ref=msgB.at[(1 - tp) * N + me],
+        dst_ref=recvB.at[here_b],
+        send_sem=ss.at[1],
+        recv_sem=rs.at[1],
+        device_id={"tp": 1 - tp},
+        device_id_type=MESH,
+    ).start()
+    step_col = jnp.sum(
+        jnp.where(iota((64, 128), 1) == me, u[160:224], 0.0), axis=1, keepdims=True
+    )
+    step_row = jnp.sum(jnp.where(diag, step_col, 0.0), axis=0, keepdims=True)
+    sumA[0:1, 0:64] = step_row
+    sumA[1:2, :] = squares
+    own_swap = swap(0, sumA, pairA)
+    own_swap.start()
     send_all(3, lambda t: msgW.at[t], recvW)
-
-    step_pre = jnp.sum(
-        jnp.where(iota((64, 64), 0) == me, by_seq[:, 128:192], 0.0), axis=0, keepdims=True
-    )
+    own_swap.wait()
+    squares = jnp.where(iota((1, 128), 1) == me, squares + pairA[1:2], 0.0)
+    own_rms = lax.rsqrt(jnp.sum(squares, axis=1, keepdims=True) / 2048.0 + EPS)
+    step_pre = (own_rms * (step_row + pairA[0:1, 0:64])).astype(BF16).astype(F32)
     shifted = step_pre + v["bias"][...]
     step = jnp.maximum(shifted, 0.0) + jnp.log1p(jnp.exp(-jnp.abs(shifted)))
     decay = -jnp.exp(v["dlog"][...]) * step
@@ -264,8 +306,11 @@
     group = ((iota((64, 64), 0) >> 3) == (iota((64, 64), 1) >> 3)).astype(BF16)
     own_head = iota((64, 32, 64), 0) == iota((64, 32, 64), 2)
 
-    all_of(rs.at[1], recvB)
-    heads = recvB[...].reshape(64, 128)
+    parts = recvB.at[pl.ds(0, 127)]
+    pltpu.make_async_copy(parts, parts, rs.at[1]).wait()
+    heads = (recvB[0:64] + recvB[64:128]).reshape(64, 128)
+    rms = lax.rsqrt(heads[:, 96:97] / 2048.0 + EPS)
+    heads = (heads * rms).astype(BF16).astype(F32)
     placed = jnp.where(here, dot(heads.astype(BF16), spread), 0.0).astype(BF16)
     maps = dot(group, placed)
     readout = silu(cio[0] + cio[1] * maps[:, 0:128]).astype(BF16)
@@ -326,21 +371,35 @@
     mixed = mixed * lax.rsqrt((squares + pairC[8:16]) / 4096.0 + EPS)
     mid = (x_own + mixed).astype(BF16)
     srcE[...] = mid
-    bufE[tp, me] = mid
-    send_all(4, lambda t: srcE, bufE.at[tp])
-    y, rms = gathered(4, srcE, bufE)
-    u = dot(we[...], y) * rms
-    act = silu(u[0:96]) * u[96:192]
-    zero = jnp.zeros((96, 64), F32)
+    bufE[me] = mid
+    send_all(4, lambda t: srcE, bufE)
+    for c in mine[2:]:
+        c.wait()
+    for c in swaps[2:]:
+        c.wait()
+    gain2 = v["cg"][...]
+    we[...] = jnp.zeros((192, 2048), BF16)
+    rpt[...] = jnp.zeros((128, 2048), F32)
+    for t in range(2):
+        we[t * 48 : t * 48 + 44] = (egF[t].astype(F32) * gain2).astype(BF16)
+        we[96 + t * 48 : 96 + t * 48 + 44] = (evF[t].astype(F32) * gain2).astype(BF16)
+        rpt[t * 48 : t * 48 + 44] = rpF[t].astype(F32)
+    pick(we, we2)
+    low, up = own_rows(rpt[...].T)
+    rt[:, 0:128] = low.astype(BF16)
+    rt[:, 128:256] = up.astype(BF16)
+    u, squares = gathered(4, bufE, we2)
+    own = jnp.where(
+        low_lanes,
+        u[0:96] + pltpu.roll(u[192:288], 64, 1),
+        pltpu.roll(u[96:192], 64, 1) + u[288:384],
+    )
+    u = joined(4, own, own, squares, sumE, pairE)
+    turned = pltpu.roll(u, 64, 1)
+    act = silu(jnp.where(low_lanes, u, turned)) * jnp.where(low_lanes, turned, u)
     pad = jnp.zeros((32, 128), F32)
     aa = jnp.concatenate(
-        [
-            jnp.concatenate([act, zero], axis=1),
-            pad,
-            jnp.concatenate([zero, act], axis=1),
-            pad,
-        ],
-        axis=0,
+        [jnp.where(low_lanes, act, 0.0), pad, jnp.where(low_lanes, 0.0, act), pad], axis=0
     ).astype(BF16)
     msgF[...] = dot(rt[...], aa).astype(BF16).reshape(64, 8, 128)
     recvF[me] = msgF[me]
@@ -348,8 +407,9 @@
     all_of(rs.at[5], recvF)
     end = mid.astype(F32) + jnp.sum(recvF[...].astype(F32), axis=0)
     out_ref[...] = jnp.concatenate([end[:, 0:64], end[:, 64:128]], axis=0)
-    for p, b in ((0, bufA.at[0]), (1, recvB), (2, recvC), (3, recvW), (4, bufE.at[0]), (5, recvF)):
+    for p, b in ((0, bufA), (2, recvC), (3, recvW), (4, bufE), (5, recvF)):
         all_of(ss.at[p], b)
+    pltpu.make_async_copy(parts, parts, ss.at[1]).wait()
 
 
 def shards(
@@ -387,18 +447,21 @@
         ev=expand_value.T,
         rp=reduce_proj,
     )
-    away = ("eg", "ev", "rp")
+    away = ("gate", "inner", "eg", "ev", "rp")
     near = [
         pltpu.VMEM(a.shape, a.dtype)
         for n, a in args.items()
         if n not in away
     ]
     scratch = near + [
-        pltpu.VMEM((192, 2048), BF16),
+        pltpu.VMEM((224, 2048), BF16),
+        pltpu.VMEM((448, 512), BF16),
+        pltpu.VMEM((2, 64, 2048), BF16),
         pltpu.VMEM((2, 44, 2048), BF16),
         pltpu.VMEM((2, 44, 2048), BF16),
         pltpu.VMEM((2, 44, 2048), BF16),
         pltpu.VMEM((192, 2048), BF16),
+        pltpu.VMEM((384, 512), BF16),
         pltpu.VMEM((8, 32, 256), BF16),
         pltpu.VMEM((512, 256), BF16),
         pltpu.VMEM((128, 2048), F32),
@@ -408,9 +471,13 @@
         pltpu.VMEM((2048, 256), BF16),
         pltpu.VMEM((1024, 128), F32),
         pltpu.VMEM((8, 128), BF16),
-        pltpu.VMEM((2, N, 8, 128), BF16),
-        pltpu.VMEM((N, 1, 128), F32),
-        pltpu.VMEM((N, 1, 128), F32),
+        pltpu.VMEM((N, 8, 128), BF16),
+        pltpu.VMEM((2 * N, 1, 128), F32),
+        pltpu.VMEM((2 * N, 1, 128), F32),
+        pltpu.VMEM((8, 128), F32),
+        pltpu.VMEM((8, 128), F32),
+        pltpu.VMEM((104, 128), F32),
+        pltpu.VMEM((104, 128), F32),
         pltpu.VMEM((16, 128), BF16),
         pltpu.VMEM((N, 16, 128), BF16),
         pltpu.VMEM((16, 128), F32),
@@ -418,13 +485,13 @@
         pltpu.VMEM((N, 8, 128), BF16),
         pltpu.VMEM((N, 8, 128), BF16),
         pltpu.VMEM((8, 128), BF16),
-        pltpu.VMEM((2, N, 8, 128), BF16),
+        pltpu.VMEM((N, 8, 128), BF16),
         pltpu.VMEM((N, 8, 128), BF16),
         pltpu.VMEM((N, 8, 128), BF16),
         pltpu.SemaphoreType.DMA((len(near),)),
-        pltpu.SemaphoreType.DMA((3,)),
-        pltpu.SemaphoreType.DMA((3,)),
-        pltpu.SemaphoreType.DMA((3,)),
+        pltpu.SemaphoreType.DMA((5,)),
+        pltpu.SemaphoreType.DMA((5,)),
+        pltpu.SemaphoreType.DMA((5,)),
         pltpu.SemaphoreType.DMA((6,)),
         pltpu.SemaphoreType.DMA((6,)),
         pltpu.SemaphoreType.DMA((6,)),

time: 63.9 us -> 60.5 us (0.947)
  Pallas kernels: 62.5 us -> 59.1 us
    pallas_call x1, Pallas kernels: 62.5 us -> 59.1 us  [shards(): pl.pallas_call(kernel, out_shape=pltpu.VMEM((16, 64), F32), in_specs=spac...]
where the time goes in v3:
time: 60.5 us; the launch traced here: 60.3 us
  Pallas kernels  59.1 us (98%)
  between operations  0.66 us (1%)
    pallas_call x1, Pallas kernels, shards(): pl.pallas_call(kernel, out_shape=pltpu.VMEM((16, 64), F32), in_specs=spac...  59.1 us

profile of v3, /device:TPU:1, one launch (start us, length us, event | category | flops | bytes accessed | tf_op | source)
XLA Modules:
  0.0 60.3 jit_solution(16642404510235523801)
XLA Ops:
  0.7 59.1 %shard_map.253 = f32[16,64]{1,0:T(8,128)S(1)} custom-call(bf16[16,64]{1,0:T(8,128)(2,1)} %refs_0_.1, f32[1,2048]{1,0:T(1,128)} %bitcast.49, bf16[32,2048]{1,0:T(8,128)(2,1)} %bitcast.40, bf16[32,2048]{1,0:T(8,128)(2,1)} %bitcast.41, bf16[16,2048]{1,0:T(8,128)(2,1)} %bitcast.43, bf16[16,2048]{1,0:T(8,128)(2,1)} %bitcast.44, bf16[64,2048]{1,0:T(8,128)(2,1)} %bitcast.36, ...), custom_call_target="tpu_custom_call" | custom-call | tf_op jit(solution)/shard_map/pallas_call | solution.py:503
  59.7 0.6 convert_element_type.3

commit v4 on v3

--- a/solution.py
+++ b/solution.py
@@ -76,7 +76,7 @@
     v = dict(zip(local, rest))
     (
         wfull, wproj, giF, egF, evF, rpF, we, we2, wd, rt, rpt, cio, cpi, msuf, s2, gf,
-        srcA, bufA, msgB, recvB, sumA, pairA, sumE, pairE, srcC, recvC, sumC, pairC, msgW, recvW, srcE, bufE, msgF, recvF,
+        srcA, bufA, msgB, recvB, sumA, pairA, otherA, sumF, pairF, srcC, recvC, sumC, pairC, msgW, recvW, srcE, bufE, msgF, recvF,
         lsem, csem, xs, xr, ss, rs, ps, pr,
     ) = rest[len(local) :]
     me, tp = lax.axis_index("kv"), lax.axis_index("tp")
@@ -147,6 +147,8 @@
     pl.semaphore_wait(barrier, N)
 
     send_all(0, lambda t: srcA, bufA)
+    hid_swap = swap(5, srcA, otherA)
+    hid_swap.start()
     swaps = [
         pltpu.make_async_remote_copy(
             src_ref=h[n],
@@ -170,10 +172,12 @@
     wfull[160:224] = (v["stepw"][...].astype(F32) * gain).astype(BF16)
     low_lanes = iota((1, 128), 1) < 64
     to, at = iota((512, 256), 0), iota((512, 256), 1)
-    spot = ((at & 127) >> 3) * 32 + 16 * tp + (at >> 7) * 8 + (at & 7)
-    picked = (to == spot).astype(BF16)
-
-    def pick(whole, out):
+    spot = ((at & 127) >> 3) * 32 + (at >> 7) * 8 + (at & 7)
+
+    def picked_of(t):
+        return (to == spot + 16 * t).astype(BF16)
+
+    def pick(whole, out, picked):
         n = whole.shape[0]
         for i in range(4):
             y = dot(whole[:, i * 512 : (i + 1) * 512], picked).astype(BF16)
@@ -186,7 +190,7 @@
         c.wait()
     for t in range(2):
         wfull[t * 64 : t * 64 + 64] = (giF[t].astype(F32) * gain).astype(BF16)
-    pick(wfull, wproj)
+    pick(wfull, wproj, picked_of(tp))
 
     for a, (t, r) in enumerate((("tout", "rout"), ("tin", "rin"))):
         taps, rec = v[t][...], v[r][...].astype(F32)
@@ -224,26 +228,12 @@
     msgW[...] = packed.astype(BF16).reshape(64, 8, 128)
     recvW[me] = msgW[me]
 
-    def own_rows(x):
-        x = x.reshape(64, 2, 16, x.shape[-1])
-        x = jnp.where(first, x[:, 0], x[:, 1])
-        return x[:, :8].reshape(512, -1), x[:, 8:].reshape(512, -1)
-
     def gathered(p, buf, w):
         all_of(rs.at[p], buf)
         x = buf[...].astype(F32)
         squares = jnp.sum(jnp.sum(x * x, axis=0), axis=0, keepdims=True)
         squares = squares + pltpu.roll(squares, 64, 1)
         return dot(w[...], x.reshape(512, 128).astype(BF16)), squares
-
-    def joined(p, own, other, squares, source, target):
-        source[0:96] = other
-        source[96:104] = jnp.broadcast_to(squares, (8, 128))
-        c = swap(p, source, target)
-        c.start()
-        c.wait()
-        squares = squares + target[96:97]
-        return (own + target[0:96]) * lax.rsqrt(squares / 2048.0 + EPS)
 
     u, squares = gathered(0, bufA, wproj)
     u = u[0:224] + pltpu.roll(u[224:448], 64, 1)
@@ -362,52 +352,89 @@
     squares = jnp.sum(jnp.where(diag, squares, 0.0), axis=0, keepdims=True)
     squares = jnp.broadcast_to(jnp.concatenate([squares, squares], axis=1), (8, 128))
     part0, part1 = halves(partial[0:16]), halves(partial[16:32])
-    sumC[0:8] = jnp.where(first, part1, part0)
-    sumC[8:16] = squares
-    c = swap(2, sumC, pairC)
-    c.start()
-    c.wait()
-    mixed = jnp.where(first, part0, part1) + pairC[0:8]
-    mixed = mixed * lax.rsqrt((squares + pairC[8:16]) / 4096.0 + EPS)
-    mid = (x_own + mixed).astype(BF16)
-    srcE[...] = mid
-    bufE[me] = mid
-    send_all(4, lambda t: srcE, bufE)
-    for c in mine[2:]:
-        c.wait()
+    hid_swap.wait()
     for c in swaps[2:]:
-        c.wait()
-    gain2 = v["cg"][...]
-    we[...] = jnp.zeros((192, 2048), BF16)
-    rpt[...] = jnp.zeros((128, 2048), F32)
-    for t in range(2):
-        we[t * 48 : t * 48 + 44] = (egF[t].astype(F32) * gain2).astype(BF16)
-        we[96 + t * 48 : 96 + t * 48 + 44] = (evF[t].astype(F32) * gain2).astype(BF16)
-        rpt[t * 48 : t * 48 + 44] = rpF[t].astype(F32)
-    pick(we, we2)
-    low, up = own_rows(rpt[...].T)
-    rt[:, 0:128] = low.astype(BF16)
-    rt[:, 128:256] = up.astype(BF16)
-    u, squares = gathered(4, bufE, we2)
-    own = jnp.where(
-        low_lanes,
-        u[0:96] + pltpu.roll(u[192:288], 64, 1),
-        pltpu.roll(u[96:192], 64, 1) + u[288:384],
-    )
-    u = joined(4, own, own, squares, sumE, pairE)
-    turned = pltpu.roll(u, 64, 1)
-    act = silu(jnp.where(low_lanes, u, turned)) * jnp.where(low_lanes, turned, u)
-    pad = jnp.zeros((32, 128), F32)
-    aa = jnp.concatenate(
-        [jnp.where(low_lanes, act, 0.0), pad, jnp.where(low_lanes, 0.0, act), pad], axis=0
-    ).astype(BF16)
-    msgF[...] = dot(rt[...], aa).astype(BF16).reshape(64, 8, 128)
-    recvF[me] = msgF[me]
-    send_all(5, lambda t: msgF.at[t], recvF)
-    all_of(rs.at[5], recvF)
-    end = mid.astype(F32) + jnp.sum(recvF[...].astype(F32), axis=0)
-    out_ref[...] = jnp.concatenate([end[:, 0:64], end[:, 64:128]], axis=0)
-    for p, b in ((0, bufA), (2, recvC), (3, recvW), (4, bufE), (5, recvF)):
+        c.wait_recv()
+
+    def unpacked(x):
+        return jnp.concatenate([x[:, 0:64], x[:, 64:128]], axis=0)
+
+    @pl.when(tp == 0)
+    def _():
+        sumC[0:8] = part0
+        sumC[8:16] = part1
+        sumC[16:24] = squares
+        c = swap(2, sumC, pairC)
+        c.start()
+        c.wait_send()
+        pltpu.make_async_copy(pairF, pairF, pr.at[4]).wait()
+        out_ref[...] = unpacked(pairF[...])
+
+    @pl.when(tp == 1)
+    def _():
+        pltpu.make_async_copy(pairC, pairC, pr.at[2]).wait()
+        scale = lax.rsqrt((squares + pairC[16:24]) / 4096.0 + EPS)
+        mids = []
+        for t, (x, part) in enumerate(((otherA[...].astype(F32), part0), (x_own, part1))):
+            mids.append((x + (part + pairC[t * 8 : t * 8 + 8]) * scale).astype(BF16))
+            srcE[t] = mids[t]
+            bufE[me, t] = mids[t]
+        send_all(4, lambda t: srcE, bufE)
+        for c in mine[2:]:
+            c.wait()
+        gain2 = v["cg"][...]
+        we[...] = jnp.zeros((192, 2048), BF16)
+        rpt[...] = jnp.zeros((128, 2048), F32)
+        for t in range(2):
+            we[t * 48 : t * 48 + 44] = (egF[t].astype(F32) * gain2).astype(BF16)
+            we[96 + t * 48 : 96 + t * 48 + 44] = (evF[t].astype(F32) * gain2).astype(BF16)
+            rpt[t * 48 : t * 48 + 44] = rpF[t].astype(F32)
+        by_row = rpt[...].T.reshape(64, 4, 8, 128)
+        for t in range(2):
+            pick(we, we2.at[t], picked_of(t))
+            for b in range(2):
+                part = by_row[:, 2 * t + b].reshape(512, 128)
+                rt[t, :, b * 128 : (b + 1) * 128] = part.astype(BF16)
+        all_of(rs.at[4], bufE)
+        y = bufE[...].astype(F32)
+        squares2 = jnp.sum(jnp.sum(y * y, axis=(0, 1)), axis=0, keepdims=True)
+        squares2 = squares2 + pltpu.roll(squares2, 64, 1)
+        u = dot(we2[0], y[:, 0].reshape(512, 128).astype(BF16))
+        u = u + dot(we2[1], y[:, 1].reshape(512, 128).astype(BF16))
+        u = jnp.where(
+            low_lanes,
+            u[0:96] + pltpu.roll(u[192:288], 64, 1),
+            pltpu.roll(u[96:192], 64, 1) + u[288:384],
+        )
+        u = u * lax.rsqrt(squares2 / 2048.0 + EPS)
+        turned = pltpu.roll(u, 64, 1)
+        act = silu(jnp.where(low_lanes, u, turned)) * jnp.where(low_lanes, turned, u)
+        pad = jnp.zeros((32, 128), F32)
+        aa = jnp.concatenate(
+            [jnp.where(low_lanes, act, 0.0), pad, jnp.where(low_lanes, 0.0, act), pad], axis=0
+        ).astype(BF16)
+        for t in range(2):
+            msgF[:, t] = dot(rt[t], aa).astype(BF16).reshape(64, 8, 128)
+        recvF[me] = msgF[me]
+        send_all(5, lambda t: msgF.at[t], recvF)
+        all_of(rs.at[5], recvF)
+        tot = jnp.sum(recvF[...].astype(F32), axis=0)
+        sumF[...] = mids[0].astype(F32) + tot[0]
+        c = swap(4, sumF, pairF)
+        c.start()
+        out_ref[...] = unpacked(mids[1].astype(F32) + tot[1])
+        c.wait_send()
+        all_of(ss.at[4], bufE)
+        all_of(ss.at[5], recvF)
+
+    @pl.when(tp == 0)
+    def _():
+        for c in mine[2:]:
+            c.wait()
+
+    for c in swaps[2:]:
+        c.wait_send()
+    for p, b in ((0, bufA), (2, recvC), (3, recvW)):
         all_of(ss.at[p], b)
     pltpu.make_async_copy(parts, parts, ss.at[1]).wait()
 
@@ -461,9 +488,9 @@
         pltpu.VMEM((2, 44, 2048), BF16),
         pltpu.VMEM((2, 44, 2048), BF16),
         pltpu.VMEM((192, 2048), BF16),
-        pltpu.VMEM((384, 512), BF16),
+        pltpu.VMEM((2, 384, 512), BF16),
         pltpu.VMEM((8, 32, 256), BF16),
-        pltpu.VMEM((512, 256), BF16),
+        pltpu.VMEM((2, 512, 256), BF16),
         pltpu.VMEM((128, 2048), F32),
         pltpu.VMEM((4, 64, 128), F32),
         pltpu.VMEM((32, 64), F32),
@@ -476,18 +503,19 @@
         pltpu.VMEM((2 * N, 1, 128), F32),
         pltpu.VMEM((8, 128), F32),
         pltpu.VMEM((8, 128), F32),
-        pltpu.VMEM((104, 128), F32),
-        pltpu.VMEM((104, 128), F32),
+        pltpu.VMEM((8, 128), BF16),
+        pltpu.VMEM((8, 128), F32),
+        pltpu.VMEM((8, 128), F32),
         pltpu.VMEM((16, 128), BF16),
         pltpu.VMEM((N, 16, 128), BF16),
-        pltpu.VMEM((16, 128), F32),
-        pltpu.VMEM((16, 128), F32),
+        pltpu.VMEM((24, 128), F32),
+        pltpu.VMEM((24, 128), F32),
         pltpu.VMEM((N, 8, 128), BF16),
         pltpu.VMEM((N, 8, 128), BF16),
-        pltpu.VMEM((8, 128), BF16),
-        pltpu.VMEM((N, 8, 128), BF16),
-        pltpu.VMEM((N, 8, 128), BF16),
-        pltpu.VMEM((N, 8, 128), BF16),
+        pltpu.VMEM((2, 8, 128), BF16),
+        pltpu.VMEM((N, 2, 8, 128), BF16),
+        pltpu.VMEM((N, 2, 8, 128), BF16),
+        pltpu.VMEM((N, 2, 8, 128), BF16),
         pltpu.SemaphoreType.DMA((len(near),)),
         pltpu.SemaphoreType.DMA((5,)),
         pltpu.SemaphoreType.DMA((5,)),

time: 60.5 us -> 59.8 us (0.988)
  Pallas kernels: 59.1 us -> 58.4 us
    pallas_call x1, Pallas kernels: 59.1 us -> 58.4 us  [shards(): pl.pallas_call(kernel, out_shape=pltpu.VMEM((16, 64), F32), in_specs=spac...]
where the time goes in v4:
time: 59.8 us; the launch traced here: 59.7 us
  Pallas kernels  58.4 us (98%)
  between operations  0.66 us (1%)
  other arithmetic  0.6 us (1%)
    pallas_call x1, Pallas kernels, shards(): pl.pallas_call(kernel, out_shape=pltpu.VMEM((16, 64), F32), in_specs=spac...  58.4 us

profile of v4, /device:TPU:1, one launch (start us, length us, event | category | flops | bytes accessed | tf_op | source)
XLA Modules:
  0.0 59.7 jit_solution(8206676937089201968)
XLA Ops:
  0.7 58.4 %shard_map.253 = f32[16,64]{1,0:T(8,128)S(1)} custom-call(bf16[16,64]{1,0:T(8,128)(2,1)} %refs_0_.1, f32[1,2048]{1,0:T(1,128)} %bitcast.49, bf16[32,2048]{1,0:T(8,128)(2,1)} %bitcast.40, bf16[32,2048]{1,0:T(8,128)(2,1)} %bitcast.41, bf16[16,2048]{1,0:T(8,128)(2,1)} %bitcast.43, bf16[16,2048]{1,0:T(8,128)(2,1)} %bitcast.44, bf16[64,2048]{1,0:T(8,128)(2,1)} %bitcast.36, ...), custom_call_target="tpu_custom_call" | custom-call | tf_op jit(solution)/shard_map/pallas_call | solution.py:531
  59.1 0.6 convert_element_type.3

commit v5 on v4

--- a/solution.py
+++ b/solution.py
@@ -76,11 +76,11 @@
     v = dict(zip(local, rest))
     (
         wfull, wproj, giF, egF, evF, rpF, we, we2, wd, rt, rpt, cio, cpi, msuf, s2, gf,
-        srcA, bufA, msgB, recvB, sumA, pairA, otherA, sumF, pairF, srcC, recvC, sumC, pairC, msgW, recvW, srcE, bufE, msgF, recvF,
+        srcA, bufA, msgB, recvB, sumA, pairA, otherA, sumF, pairF, srcC, recvC, msgW, recvW, srcE, bufE, msgF, recvF,
         lsem, csem, xs, xr, ss, rs, ps, pr,
     ) = rest[len(local) :]
     me, tp = lax.axis_index("kv"), lax.axis_index("tp")
-    first = tp == 0
+    here_b = tp * N + me
 
     order = (4, 3, 5, 2, 6, 1, 7, 0)
     in_rows = [lax.rem(me // 8 + o, 8) * 8 for o in order]
@@ -125,6 +125,28 @@
 
         for t in peers:
             one(t, 0)
+
+    def to_last(p, source, target):
+        def one(t):
+            pltpu.make_async_remote_copy(
+                src_ref=source(me if t is None else t),
+                dst_ref=target.at[here_b],
+                send_sem=ss.at[p],
+                recv_sem=rs.at[p],
+                device_id={"tp": 1} if t is None else {"kv": t, "tp": 1},
+                device_id_type=MESH,
+            ).start()
+
+        for t in peers:
+            one(t)
+
+        @pl.when(tp == 0)
+        def _():
+            one(None)
+
+    def count(sem, buf, n):
+        some = buf.at[pl.ds(0, n)]
+        pltpu.make_async_copy(some, some, sem).wait()
 
     def all_of(sem, buf):
         most = buf.at[pl.ds(0, N - 1)]
@@ -226,7 +248,7 @@
     for q in range(1, 4):
         packed = packed + pltpu.roll(rows[:, q].reshape(512, 128), 32 * q, 1)
     msgW[...] = packed.astype(BF16).reshape(64, 8, 128)
-    recvW[me] = msgW[me]
+    recvW[here_b] = msgW[me]
 
     def gathered(p, buf, w):
         all_of(rs.at[p], buf)
@@ -243,7 +265,6 @@
     by_core = [jnp.concatenate([u[t * 64 : t * 64 + 64], tail], axis=0) for t in range(2)]
     by_seq = jnp.where(low_lanes, by_core[0], pltpu.roll(by_core[1], 64, 1)).T
     msgB[...] = by_seq.reshape(128, 1, 128)
-    here_b = tp * N + me
     recvB[here_b] = msgB[here_b]
 
     def send_parts(i, c):
@@ -277,7 +298,7 @@
     sumA[1:2, :] = squares
     own_swap = swap(0, sumA, pairA)
     own_swap.start()
-    send_all(3, lambda t: msgW.at[t], recvW)
+    to_last(3, lambda t: msgW.at[t], recvW)
     own_swap.wait()
     squares = jnp.where(iota((1, 128), 1) == me, squares + pairA[1:2], 0.0)
     own_rms = lax.rsqrt(jnp.sum(squares, axis=1, keepdims=True) / 2048.0 + EPS)
@@ -326,32 +347,9 @@
     for q in range(1, 4):
         packed = packed + pltpu.roll(by_head[q * 16 : (q + 1) * 16], 32 * q, 1)
     srcC[...] = packed.astype(BF16)
-    recvC[me] = packed.astype(BF16)
-    send_all(2, lambda t: srcC, recvC)
-
-    all_of(rs.at[3], recvW)
-    tiles = recvW[...].astype(F32).reshape(4, 128, 128)
-    block = iota((128, 128), 1) >> 5
-    for dd in range(4):
-        out = jnp.zeros((128, 128), F32)
-        for q in range(4):
-            turned = tiles[q] if q == dd else pltpu.roll(tiles[q], (32 * (q - dd)) % 128, 1)
-            out = jnp.where(block == q, turned, out)
-        out = out.astype(BF16).reshape(16, 8, 128)
-        for i in range(16):
-            wd[i // 2, dd * 8 : dd * 8 + 8, (i % 2) * 128 : (i % 2) * 128 + 128] = out[i]
-
-    all_of(rs.at[2], recvC)
-    gates = recvC[...].astype(F32)
-    gf[...] = gates.reshape(1024, 128)
-    partial = jnp.zeros((32, 64), F32)
-    for i in range(8):
-        pair = [gf[pl.ds(2 * i + e, 64, stride=16), :] for e in range(2)]
-        partial = partial + dot_t(wd[i], jnp.concatenate(pair, axis=1).astype(BF16))
-    squares = jnp.sum(jnp.sum(gates * gates, axis=1), axis=1, keepdims=True)
-    squares = jnp.sum(jnp.where(diag, squares, 0.0), axis=0, keepdims=True)
-    squares = jnp.broadcast_to(jnp.concatenate([squares, squares], axis=1), (8, 128))
-    part0, part1 = halves(partial[0:16]), halves(partial[16:32])
+    recvC[here_b] = packed.astype(BF16)
+    to_last(2, lambda t: srcC, recvC)
+
     hid_swap.wait()
     for c in swaps[2:]:
         c.wait_recv()
@@ -361,22 +359,44 @@
 
     @pl.when(tp == 0)
     def _():
-        sumC[0:8] = part0
-        sumC[8:16] = part1
-        sumC[16:24] = squares
-        c = swap(2, sumC, pairC)
-        c.start()
-        c.wait_send()
         pltpu.make_async_copy(pairF, pairF, pr.at[4]).wait()
         out_ref[...] = unpacked(pairF[...])
 
     @pl.when(tp == 1)
     def _():
-        pltpu.make_async_copy(pairC, pairC, pr.at[2]).wait()
-        scale = lax.rsqrt((squares + pairC[16:24]) / 4096.0 + EPS)
+        count(rs.at[3], recvW, 127)
+        tiles = recvW[...].astype(F32).reshape(8, 128, 128)
+        block = iota((128, 128), 1) >> 5
+        for t in range(2):
+            for dd in range(4):
+                out = jnp.zeros((128, 128), F32)
+                for q in range(4):
+                    turned = tiles[t * 4 + q]
+                    if q != dd:
+                        turned = pltpu.roll(turned, (32 * (q - dd)) % 128, 1)
+                    out = jnp.where(block == q, turned, out)
+                out = out.astype(BF16).reshape(16, 8, 128)
+                for i in range(16):
+                    lanes = slice((i % 2) * 128, (i % 2) * 128 + 128)
+                    wd[t * 8 + i // 2, dd * 8 : dd * 8 + 8, lanes] = out[i]
+        count(rs.at[2], recvC, 127)
+        gates = recvC[...].astype(F32)
+        gf[...] = gates.reshape(2048, 128)
+        partial = jnp.zeros((32, 64), F32)
+        for t in range(2):
+            for i in range(8):
+                pair = [gf[pl.ds(t * 1024 + 2 * i + e, 64, stride=16), :] for e in range(2)]
+                pair = jnp.concatenate(pair, axis=1).astype(BF16)
+                partial = partial + dot_t(wd[t * 8 + i], pair)
+        squares = jnp.sum(jnp.sum(gates * gates, axis=1), axis=1, keepdims=True)
+        squares = squares[0:64] + squares[64:128]
+        squares = jnp.sum(jnp.where(diag, squares, 0.0), axis=0, keepdims=True)
+        squares = jnp.concatenate([squares, squares], axis=1)
+        part0, part1 = halves(partial[0:16]), halves(partial[16:32])
+        scale = lax.rsqrt(squares / 4096.0 + EPS)
         mids = []
         for t, (x, part) in enumerate(((otherA[...].astype(F32), part0), (x_own, part1))):
-            mids.append((x + (part + pairC[t * 8 : t * 8 + 8]) * scale).astype(BF16))
+            mids.append((x + part * scale).astype(BF16))
             srcE[t] = mids[t]
             bufE[me, t] = mids[t]
         send_all(4, lambda t: srcE, bufE)
@@ -431,11 +451,18 @@
     def _():
         for c in mine[2:]:
             c.wait()
+        count(ss.at[2], recvC, 64)
+        count(ss.at[3], recvW, 64)
 
     for c in swaps[2:]:
         c.wait_send()
-    for p, b in ((0, bufA), (2, recvC), (3, recvW)):
-        all_of(ss.at[p], b)
+
+    @pl.when(tp == 1)
+    def _():
+        count(ss.at[2], recvC, 63)
+        count(ss.at[3], recvW, 63)
+
+    all_of(ss.at[0], bufA)
     pltpu.make_async_copy(parts, parts, ss.at[1]).wait()
 
 
@@ -489,14 +516,14 @@
         pltpu.VMEM((2, 44, 2048), BF16),
         pltpu.VMEM((192, 2048), BF16),
         pltpu.VMEM((2, 384, 512), BF16),
-        pltpu.VMEM((8, 32, 256), BF16),
+        pltpu.VMEM((16, 32, 256), BF16),
         pltpu.VMEM((2, 512, 256), BF16),
         pltpu.VMEM((128, 2048), F32),
         pltpu.VMEM((4, 64, 128), F32),
         pltpu.VMEM((32, 64), F32),
         pltpu.VMEM((64, 128), F32),
         pltpu.VMEM((2048, 256), BF16),
-        pltpu.VMEM((1024, 128), F32),
+        pltpu.VMEM((2048, 128), F32),
         pltpu.VMEM((8, 128), BF16),
         pltpu.VMEM((N, 8, 128), BF16),
         pltpu.VMEM((2 * N, 1, 128), F32),
@@ -507,11 +534,9 @@
         pltpu.VMEM((8, 128), F32),
         pltpu.VMEM((8, 128), F32),
         pltpu.VMEM((16, 128), BF16),
-        pltpu.VMEM((N, 16, 128), BF16),
-        pltpu.VMEM((24, 128), F32),
-        pltpu.VMEM((24, 128), F32),
+        pltpu.VMEM((2 * N, 16, 128), BF16),
         pltpu.VMEM((N, 8, 128), BF16),
-        pltpu.VMEM((N, 8, 128), BF16),
+        pltpu.VMEM((2 * N, 8, 128), BF16),
         pltpu.VMEM((2, 8, 128), BF16),
         pltpu.VMEM((N, 2, 8, 128), BF16),
         pltpu.VMEM((N, 2, 8, 128), BF16),

time: 59.8 us -> 58.9 us (0.985)
  Pallas kernels: 58.4 us -> 57.5 us
    pallas_call x1, Pallas kernels: 58.4 us -> 57.5 us  [shards(): pl.pallas_call(kernel, out_shape=pltpu.VMEM((16, 64), F32), in_specs=spac...]
where the time goes in v5:
time: 58.9 us; the launch traced here: 58.8 us
  Pallas kernels  57.5 us (98%)
  between operations  0.66 us (1%)
  other arithmetic  0.6 us (1%)
    pallas_call x1, Pallas kernels, shards(): pl.pallas_call(kernel, out_shape=pltpu.VMEM((16, 64), F32), in_specs=spac...  57.5 us

profile of v5, /device:TPU:1, one launch (start us, length us, event | category | flops | bytes accessed | tf_op | source)
XLA Modules:
  0.0 58.8 jit_solution(2986695241962692156)
XLA Ops:
  0.7 57.5 %shard_map.253 = f32[16,64]{1,0:T(8,128)S(1)} custom-call(bf16[16,64]{1,0:T(8,128)(2,1)} %refs_0_.1, f32[1,2048]{1,0:T(1,128)} %bitcast.49, bf16[32,2048]{1,0:T(8,128)(2,1)} %bitcast.40, bf16[32,2048]{1,0:T(8,128)(2,1)} %bitcast.41, bf16[16,2048]{1,0:T(8,128)(2,1)} %bitcast.43, bf16[16,2048]{1,0:T(8,128)(2,1)} %bitcast.44, bf16[64,2048]{1,0:T(8,128)(2,1)} %bitcast.36, ...), custom_call_target="tpu_custom_call" | custom-call | tf_op jit(solution)/shard_map/pallas_call | solution.py:556
  58.2 0.6 %convert_element_type.3 = bf16[16,64]{1,0:T(8,128)(2,1)} convert(f32[16,64]{1,0:T(8,128)S(1)} %shard_map.253) | non-fusion elementwise | flops 1024 | bytes 6144 | tf_op jit(solution)/shard_map/convert_element_type | solution.py:564

commit v6 on v5

--- a/solution.py
+++ b/solution.py
@@ -298,7 +298,6 @@
     sumA[1:2, :] = squares
     own_swap = swap(0, sumA, pairA)
     own_swap.start()
-    to_last(3, lambda t: msgW.at[t], recvW)
     own_swap.wait()
     squares = jnp.where(iota((1, 128), 1) == me, squares + pairA[1:2], 0.0)
     own_rms = lax.rsqrt(jnp.sum(squares, axis=1, keepdims=True) / 2048.0 + EPS)
@@ -316,6 +315,7 @@
     here = ((iota((64, 256), 1) & 127) >> 4) == (iota((64, 256), 0) & 7)
     group = ((iota((64, 64), 0) >> 3) == (iota((64, 64), 1) >> 3)).astype(BF16)
     own_head = iota((64, 32, 64), 0) == iota((64, 32, 64), 2)
+    to_last(3, lambda t: msgW.at[t], recvW)
 
     parts = recvB.at[pl.ds(0, 127)]
     pltpu.make_async_copy(parts, parts, rs.at[1]).wait()
@@ -438,11 +438,10 @@
         recvF[me] = msgF[me]
         send_all(5, lambda t: msgF.at[t], recvF)
         all_of(rs.at[5], recvF)
-        tot = jnp.sum(recvF[...].astype(F32), axis=0)
-        sumF[...] = mids[0].astype(F32) + tot[0]
+        sumF[...] = mids[0].astype(F32) + jnp.sum(recvF[:, 0].astype(F32), axis=0)
         c = swap(4, sumF, pairF)
         c.start()
-        out_ref[...] = unpacked(mids[1].astype(F32) + tot[1])
+        out_ref[...] = unpacked(mids[1].astype(F32) + jnp.sum(recvF[:, 1].astype(F32), axis=0))
         c.wait_send()
         all_of(ss.at[4], bufE)
         all_of(ss.at[5], recvF)

time: 58.9 us -> 58.8 us (level)
  no operation moved by 1% of the time
where the time goes in v6:
time: 58.8 us; the launch traced here: 58.6 us
  Pallas kernels  57.4 us (98%)
  between operations  0.66 us (1%)
  other arithmetic  0.6 us (1%)
    pallas_call x1, Pallas kernels, shards(): pl.pallas_call(kernel, out_shape=pltpu.VMEM((16, 64), F32), in_specs=spac...  57.4 us

profile of v6, /device:TPU:1, one launch (start us, length us, event | category | flops | bytes accessed | tf_op | source)
XLA Modules:
  0.0 58.6 jit_solution(13191628199014364991)
XLA Ops:
  0.7 57.4 %shard_map.253 = f32[16,64]{1,0:T(8,128)S(1)} custom-call(bf16[16,64]{1,0:T(8,128)(2,1)} %refs_0_.1, f32[1,2048]{1,0:T(1,128)} %bitcast.49, bf16[32,2048]{1,0:T(8,128)(2,1)} %bitcast.40, bf16[32,2048]{1,0:T(8,128)(2,1)} %bitcast.41, bf16[16,2048]{1,0:T(8,128)(2,1)} %bitcast.43, bf16[16,2048]{1,0:T(8,128)(2,1)} %bitcast.44, bf16[64,2048]{1,0:T(8,128)(2,1)} %bitcast.36, ...), custom_call_target="tpu_custom_call" | custom-call | tf_op jit(solution)/shard_map/pallas_call | solution.py:555
  58.0 0.6 %convert_element_type.3 = bf16[16,64]{1,0:T(8,128)(2,1)} convert(f32[16,64]{1,0:T(8,128)S(1)} %shard_map.253) | non-fusion elementwise | flops 1024 | bytes 6144 | tf_op jit(solution)/shard_map/convert_element_type | solution.py:563
